TPU v7x, 128 devices: a whole 4x4x4 slice. The times are simulated.
128 devices in a mesh: fs: 16 (over z, x), tp: 8 (over y, core).
Axes of the slice: x: 4, y: 4, z: 4, core: 2. Of those that a mesh axis runs over, the one named last changes fastest.
Arguments:
- tokens: bfloat16 [16384, 2048], P(('fs', 'tp')), may hold values from -6 to 6
- mix_gain: float32 [2048], replicated, may hold values from 0.1 to 1.9
- ffn_gain: float32 [2048], replicated, may hold values from 0.1 to 1.9
- u_weight: float32 [2048, 2048], P('fs', 'tp'), may hold values from -0.125 to 0.125
- u_scale: float32 [2048], P('tp'), may hold values from 0.5 to 2
- v_weight: float32 [2048, 2048], P('fs', 'tp'), may hold values from -0.125 to 0.125
- v_scale: float32 [2048], P('tp'), may hold values from 0.3 to 12
- v_gain: float32 [2048], P('tp'), may hold values from 0.1 to 1.9
- spatial_weight: bfloat16 [8, 128, 128], replicated, may hold values from -0.5 to 0.5
- spatial_bias: float32 [8, 128], replicated, may hold values from 0.1 to 1.9
- out_weight: float32 [2048, 2048], P('tp', 'fs'), may hold values from -0.125 to 0.125
- out_scale: float32 [2048], P('fs'), may hold values from 0.5 to 2
- gate_weight: float32 [2048, 6144], P('fs', 'tp'), may hold values from -0.125 to 0.125
- gate_scale: float32 [6144], P('tp'), may hold values from 0.5 to 2
- up_weight: float32 [2048, 6144], P('fs', 'tp'), may hold values from -0.125 to 0.125
- up_scale: float32 [6144], P('tp'), may hold values from 0.5 to 2
- down_weight: float32 [6144, 2048], P('tp', 'fs'), may hold values from -0.078125 to 0.078125
- down_scale: float32 [2048], P('fs'), may hold values from 0.5 to 2
Outputs:
- layer_out: bfloat16 [16384, 2048], P(('fs', 'tp'))
All inputs are finite; a program needn't handle non-finite values.
Results may differ from a plain program's by a relative error of at most 0.02.
Values may be sent and summed in bfloat16 or wider, within the bound.
A program may use at most 64 MiB of HBM per device.

v0:
```python
import jax
import jax.numpy as jnp
from jax import lax
from jax.sharding import Mesh
from jax.sharding import PartitionSpec as P

A = 2048
A_GROUPS = 8
BLK = 128
TP = ("tp_0", "tp_1")
FS_TP = ("fs", "tp_0", "tp_1")


def copy_for_each(value, axis):
    peers = lax.axis_size(axis)
    return lax.all_to_all(
        jnp.broadcast_to(value[None], (peers, *value.shape)), axis, 0, 0, tiled=True
    )


def laid_out(tiles, dim):
    dims = list(tiles.shape[1:])
    dims[dim] *= tiles.shape[0]
    return jnp.moveaxis(tiles, 0, dim).reshape(dims)


def gather_axes(value, axes, dim):
    far, near = axes
    tiles = copy_for_each(copy_for_each(value, far), near)
    return laid_out(tiles.swapaxes(0, 1).reshape(-1, *value.shape), dim)


def split_up(value, dim, peers):
    dims = value.shape
    tiles = value.reshape(*dims[:dim], peers, dims[dim] // peers, *dims[dim + 1 :])
    return jnp.moveaxis(tiles, dim, 0)


def sent_and_summed(value, axis, dim):
    tiles = split_up(value, dim, lax.axis_size(axis))
    arrived = lax.all_to_all(tiles, axis, split_axis=0, concat_axis=0, tiled=True)
    return arrived.astype(jnp.float32).sum(axis=0)


def sum_in_two_steps(value, axes, dim):
    far, near = axes
    own = sent_and_summed(split_up(value, dim, lax.axis_size(far)), near, dim + 1)
    return jnp.sum(
        lax.all_to_all(own.astype(jnp.bfloat16), far, 0, 0, tiled=True).astype(jnp.float32), axis=0
    )


def turned_gather(arrays, axis, dims):
    turned = [jnp.moveaxis(a, dim, 0) for a, dim in zip(arrays, dims)]
    both = jnp.concatenate([t.reshape(len(t), -1) for t in turned], axis=1)
    out, at, finished = (lax.all_gather(both, axis, axis=0, tiled=True), 0, [])
    for t, dim in zip(turned, dims):
        piece = out[:, at : at + t[0].size].reshape(-1, *t.shape[1:])
        finished.append(jnp.moveaxis(piece, 0, dim))
        at += t[0].size
    return tuple(finished)


def of_everyone(value, axis):
    return copy_for_each(value, axis).sum(axis=0)


def packed_total(arrays, axis):
    ravelled, at, finished = (jnp.concatenate([a.reshape(-1) for a in arrays]), 0, [])
    running = of_everyone(ravelled, axis)
    for a in arrays:
        finished.append(running[at : at + a.size].reshape(a.shape))
        at += a.size
    return tuple(finished)


def rms_rows(values, norm_gain):
    widened = values.astype(jnp.float32)
    factor = lax.rsqrt(jnp.mean(widened * widened, axis=1, keepdims=True) + 1e-06)
    return (widened * factor * norm_gain).astype(jnp.bfloat16)


def collect_rows(shard_rows, project):
    return project(gather_axes(shard_rows, ("tp_0", "tp_1"), 0), jnp.int32(0))


def reduce_rows(term_fn, local_rows):
    return sum_in_two_steps(
        term_fn(jnp.int32(0), local_rows * lax.axis_size(TP)).astype(jnp.bfloat16),
        ("tp_0", "tp_1"),
        0,
    )


def local(
    tokens,
    mix_gain,
    ffn_gain,
    u_weight,
    u_scale,
    v_weight,
    v_scale,
    v_gain,
    spatial_weight,
    spatial_bias,
    out_weight,
    out_scale,
    gate_weight,
    gate_scale,
    up_weight,
    up_scale,
    down_weight,
    down_scale,
):
    local_rows = tokens.shape[0]
    out_columns, down_columns = turned_gather((out_scale, down_scale), "fs", (0, 0))
    u_whole, v_whole, out_whole = turned_gather(
        (
            u_weight.astype(jnp.bfloat16),
            v_weight.astype(jnp.bfloat16),
            out_weight.astype(jnp.bfloat16),
        ),
        "fs",
        (0, 0, 1),
    )
    normed = rms_rows(tokens, mix_gain)

    def project_mixer(segment, offset):
        u_pre = jnp.dot(segment, u_whole, preferred_element_type=jnp.float32) * u_scale
        v_pre = jnp.dot(segment, v_whole, preferred_element_type=jnp.float32) * v_scale
        return jnp.concatenate(
            [jax.nn.gelu(u_pre, approximate=True), jax.nn.gelu(v_pre, approximate=True)], axis=1
        ).astype(jnp.bfloat16)

    joined = collect_rows(normed, project_mixer)
    columns = u_whole.shape[1]
    u_values = joined[:, :columns]
    v_wide = joined[:, columns:].astype(jnp.float32)
    totals, squares = packed_total((jnp.sum(v_wide, axis=1), jnp.sum(v_wide * v_wide, axis=1)), TP)
    average = totals / A
    spread = squares / A - average * average
    v_normed = ((v_wide - average[:, None]) * lax.rsqrt(spread + 1e-05)[:, None] * v_gain).astype(
        jnp.bfloat16
    )
    group_dim = A // A_GROUPS
    groups = columns // group_dim
    first_group = lax.axis_index(TP) * groups
    weights = lax.dynamic_slice_in_dim(spatial_weight, first_group, groups, 0)
    offsets = lax.dynamic_slice_in_dim(spatial_bias, first_group, groups, 0)
    causal = jnp.tril(jnp.ones((BLK, BLK), dtype=bool))
    masked = jnp.where(causal[None], weights, jnp.zeros_like(weights))
    blocks = v_normed.reshape(-1, BLK, groups, group_dim)
    mixed_sum = jnp.einsum("gts,bsgd->btgd", masked, blocks, preferred_element_type=jnp.float32)
    mixed_sum = mixed_sum + offsets.T[None, :, :, None]
    gated_rows = (u_values.reshape(blocks.shape).astype(jnp.float32) * mixed_sum).astype(
        jnp.bfloat16
    )
    gated_rows = gated_rows.reshape(-1, columns)

    def mixer_term(offset, amount):
        return jnp.dot(gated_rows, out_whole, preferred_element_type=jnp.float32) * out_columns

    residual = (tokens.astype(jnp.float32) + reduce_rows(mixer_term, local_rows)).astype(
        jnp.bfloat16
    )
    gate_whole, up_whole, down_whole = turned_gather(
        (
            gate_weight.astype(jnp.bfloat16),
            up_weight.astype(jnp.bfloat16),
            down_weight.astype(jnp.bfloat16),
        ),
        "fs",
        (0, 0, 1),
    )
    normed_second = rms_rows(residual, ffn_gain)

    def project_ffn(segment, offset):
        gate_pre = jnp.dot(segment, gate_whole, preferred_element_type=jnp.float32) * gate_scale
        up_pre = jnp.dot(segment, up_whole, preferred_element_type=jnp.float32) * up_scale
        return (jax.nn.silu(gate_pre) * up_pre).astype(jnp.bfloat16)

    hidden = collect_rows(normed_second, project_ffn)

    def ffn_term(offset, amount):
        return jnp.dot(hidden, down_whole, preferred_element_type=jnp.float32) * down_columns

    return (residual.astype(jnp.float32) + reduce_rows(ffn_term, local_rows)).astype(jnp.bfloat16)


def solution(mesh):
    torus = Mesh(mesh.devices.reshape(mesh.shape["fs"], 4, 2), ("fs", "tp_0", "tp_1"))
    in_specs = (
        P(FS_TP, None),
        P(),
        P(),
        P("fs", TP),
        P(TP),
        P("fs", TP),
        P(TP),
        P(TP),
        P(),
        P(),
        P(TP, "fs"),
        P("fs"),
        P("fs", TP),
        P(TP),
        P("fs", TP),
        P(TP),
        P(TP, "fs"),
        P("fs"),
    )
    out_specs = P(FS_TP, None)
    return jax.shard_map(local, mesh=torus, in_specs=in_specs, out_specs=out_specs, check_vma=False)
```

profile of v0, /device:TPU:0, one launch (start us, length us, event | category | flops | bytes accessed | tf_op | source)
XLA Modules:
  0.0 238.4 jit_solution(4988067022852905276)
XLA Ops:
  6.5 0.0 copy-start
  6.5 0.0 all-gather.3.cloned.1.call-start
  6.5 1.1 copy.44
  7.6 1.0 copy.45
  8.7 0.9 convert_bitcast_fusion.1
  9.6 0.7 pad_maximum_fusion.1
  10.3 0.0 all-gather.3.cloned.1.call-update
  10.3 0.0 all-gather.5.cloned.1.call-start
  10.3 1.2 copy.49
  11.5 1.2 copy.50
  12.7 1.0 convert_bitcast_fusion
  13.7 0.8 pad_maximum_fusion
  14.5 0.0 all-gather.5.cloned.1.call-update
  14.6 0.0 copy-done.2
  14.6 0.2 fusion.13
  14.8 0.0 copy-done.3
  14.8 0.2 fusion.15
  15.0 0.0 copy-start.6
  15.0 0.0 copy-start.7
  15.0 1.6 broadcast_in_dim.13
  16.6 4.6 %all-to-all-start = ((bf16[4,128,2048]{2,1,0:T(8,128)(2,1)}), bf16[4,128,2048]{2,1,0:T(8,128)(2,1)S(1)}, u32[]{:S(2)}, u32[]{:S(2)}) async-start(bf16[4,128,2048]{2,1,0:T(8,128)(2,1)} %broadcast_in_dim.13), calls=%async_computation | async-start | bytes 4194304 | tf_op jit(solution)/shard_map/all_to_all | solution.py:16
  21.1 0.0 copy-done.6
  21.1 0.0 copy-done.7
  21.2 24.7 %all_gather.10 = f32[2048,2]{0,1:T(2,128)S(1)} all-gather(f32[128,2]{0,1:T(2,128)S(1)} %pad_maximum_fusion.3), channel_id=1, replica_groups=mesh['fs'=16,'tp_0'=4,'tp_1'=2] {'fs'}, dimensions={0}, use_global_device_ids=true | all-gather | bytes 17408 | tf_op jit(solution)/shard_map/all_gather | solution.py:56
  45.9 0.0 copy-done
  45.9 1.6 all-to-all-done
  47.5 0.5 broadcast_in_dim.14
  48.0 7.1 %all_to_all.46 = bf16[2,4,128,2048]{3,2,1,0:T(8,128)(2,1)S(1)} all-to-all(bf16[2,4,128,2048]{3,2,1,0:T(8,128)(2,1)S(1)} %broadcast_in_dim.14), channel_id=1, replica_groups=mesh['fs'=16,'tp_0'=4,'tp_1'=2] {'tp_1'}, dimensions={0} | all-to-all | bytes 8388608 | tf_op jit(solution)/shard_map/all_to_all | solution.py:16
  55.1 2.4 copy.43
  57.5 7.4 %all-gather.3.cloned.1.call-done = bf16[2048,768]{0,1:T(8,128)(2,1)} async-done(((bf16[128,768]{0,1:T(8,128)(2,1)}), bf16[2048,768]{0,1:T(8,128)(2,1)}) %all-gather.3.cloned.1.call-update) | async-done | bytes 3145744 | tf_op jit(solution)/shard_map/all_gather | solution.py:56
  64.9 0.0 copy-done.10
  64.9 4.2 %convert_reduce_fusion.2 = (f32[1024]{0:T(1024)S(1)}, f32[1024]{0:T(1024)S(1)}, bf16[1024,256]{1,0:T(8,128)(2,1)S(1)}) fusion(f32[256]{0:T(256)S(1)} %copy-done.10, bf16[1024,2048]{1,0:T(8,128)(2,1)} %bitcast.56, bf16[2048,768]{0,1:T(8,128)(2,1)} %all-gather.3.cloned.1.call-done), kind=kOutput, calls=%fused_computation.17 | convolution fusion | flops 1077409792 | bytes 5776384 | tf_op jit(solution)/shard_map/dot_general | solution.py:130
  69.1 0.7 broadcast_in_dim.15
  69.7 4.3 %all-to-all-start.2 = ((f32[8,1,2048]{2,1,0:T(1,128)}), f32[8,1,2048]{2,1,0:T(1,128)S(1)}, u32[]{:S(2)}, u32[]{:S(2)}) async-start(f32[8,1,2048]{2,1,0:T(1,128)} %broadcast_in_dim.15), calls=%async_computation.2 | async-start | bytes 131072 | tf_op jit(solution)/shard_map/all_to_all | solution.py:16
  74.0 0.0 copy-done.11
  74.0 0.0 copy-start.5
  74.0 4.2 %fusion.24 = bf16[1024,256]{1,0:T(8,128)(2,1)S(1)} fusion(bf16[1024,2048]{1,0:T(8,128)(2,1)} %bitcast.57, bf16[2048,768]{0,1:T(8,128)(2,1)} %all-gather.3.cloned.1.call-done, f32[256]{0:T(256)S(1)} %copy-done.11), kind=kOutput, calls=%fused_computation.41 | convolution fusion | flops 1076363264 | bytes 5768192 | tf_op jit(solution)/shard_map/dot_general | solution.py:129
  78.3 1.4 all-to-all-done.2
  79.6 0.1 reduce_sum.90
  79.7 0.3 fusion.36
  80.1 1.0 fusion.12
  81.1 2.5 %multiply_convert_fusion.1 = bf16[1024,2048]{1,0:T(8,128)(2,1)S(1)} fusion(bf16[1024,256]{1,0:T(8,128)(2,1)S(1)} %bitcast.64, f32[2048]{0:T(1024)S(1)} %bitcast.66, bf16[2048,768]{0,1:T(8,128)(2,1)} %all-gather.3.cloned.1.call-done), kind=kOutput, calls=%fused_computation.1 | convolution fusion | flops 1077936128 | bytes 5775360 | tf_op jit(solution)/shard_map/dot_general | solution.py:161
  83.6 0.6 copy.58
  84.2 8.1 %all_to_all.47 = bf16[2,4,128,2048]{3,2,1,0:T(8,128)(2,1)} all-to-all(bf16[2,4,128,2048]{3,2,1,0:T(8,128)(2,1)S(1)} %bitcast.54), channel_id=1, replica_groups=mesh['fs'=16,'tp_0'=4,'tp_1'=2] {'tp_1'}, dimensions={0} | all-to-all | bytes 8388608 | tf_op jit(solution)/shard_map/all_to_all | solution.py:41
  92.3 3.6 %reduce_sum.91 = bf16[4,128,2048]{2,1,0:T(8,128)(2,1)S(1)} reduce(bf16[2,4,128,2048]{3,2,1,0:T(8,128)(2,1)} %all_to_all.47, bf16[]{:T(256)} %constant.43.clone.1), dimensions={0}, to_apply=%region_4.5 | reduce | flops 1048576 | bytes 6291458 | tf_op jit(solution)/shard_map/reduce_sum | solution.py:42
  95.9 30.0 %all_to_all.48 = bf16[4,128,2048]{2,1,0:T(8,128)(2,1)S(1)} all-to-all(bf16[4,128,2048]{2,1,0:T(8,128)(2,1)S(1)} %reduce_sum.91), channel_id=1, replica_groups=mesh['fs'=16,'tp_0'=4,'tp_1'=2] {'tp_0'}, dimensions={0} | all-to-all | bytes 4194304 | tf_op jit(solution)/shard_map/all_to_all | solution.py:49
  125.9 0.4 convert_reduce_fusion.1
  126.3 0.3 fusion.37
  126.5 0.0 copy-done.4
  126.6 0.2 fusion.39
  126.8 0.2 broadcast_in_dim.17
  127.0 28.0 %all_to_all.49 = bf16[4,128,2048]{2,1,0:T(8,128)(2,1)S(1)} all-to-all(bf16[4,128,2048]{2,1,0:T(8,128)(2,1)S(1)} %broadcast_in_dim.17), channel_id=1, replica_groups=mesh['fs'=16,'tp_0'=4,'tp_1'=2] {'tp_0'}, dimensions={0} | all-to-all | bytes 4194304 | tf_op jit(solution)/shard_map/all_to_all | solution.py:16
  155.0 0.5 broadcast_in_dim.18
  155.5 7.1 %all_to_all.50 = bf16[2,4,128,2048]{3,2,1,0:T(8,128)(2,1)S(1)} all-to-all(bf16[2,4,128,2048]{3,2,1,0:T(8,128)(2,1)S(1)} %broadcast_in_dim.18), channel_id=1, replica_groups=mesh['fs'=16,'tp_0'=4,'tp_1'=2] {'tp_1'}, dimensions={0} | all-to-all | bytes 8388608 | tf_op jit(solution)/shard_map/all_to_all | solution.py:16
  162.6 2.4 copy.48
  165.0 8.2 %fusion.1 = f32[1024,768]{1,0:T(8,128)} fusion(bf16[1024,2048]{1,0:T(8,128)(2,1)} %bitcast.58, bf16[2048,2304]{0,1:T(8,128)(2,1)} %all-gather.5.cloned.1.call-done), kind=kOutput, calls=%fused_computation.7 | convolution fusion | flops 3221225472 | bytes 10485760 | tf_op jit(solution)/shard_map/dot_general | solution.py:179
  173.3 13.4 %multiply_convert_fusion = bf16[1024,2048]{1,0:T(8,128)(2,1)} fusion(f32[2048]{0:T(1024)S(1)} %bitcast.65, bf16[2048,2304]{0,1:T(8,128)(2,1)} %all-gather.5.cloned.1.call-done, f32[1024,768]{1,0:T(8,128)} %fusion.1, bf16[1024,2048]{1,0:T(8,128)(2,1)} %bitcast.59, f32[768]{0:T(1024)S(1)} %copy-done.8, f32[768]{0:T(1024)S(1)} %copy-done.9), kind=kOutput, calls=%fused_computation | convolution fusion | flops 6452936704 | bytes 17840128 | tf_op jit(solution)/shard_map/dot_general | solution.py:185
  186.6 2.5 %copy.57 = bf16[4,2,128,2048]{3,2,0,1:T(8,128)(2,1)S(1)} copy(bf16[4,2,128,2048]{3,2,1,0:T(8,128)(2,1)} %bitcast.60) | data formatting | bytes 8388608 | tf_op jit(solution)/shard_map/reshape;reshape | solution.py:35
  189.1 8.2 %all_to_all.51 = bf16[2,4,128,2048]{3,2,1,0:T(8,128)(2,1)} all-to-all(bf16[2,4,128,2048]{3,2,1,0:T(8,128)(2,1)S(1)} %bitcast.55), channel_id=1, replica_groups=mesh['fs'=16,'tp_0'=4,'tp_1'=2] {'tp_1'}, dimensions={0} | all-to-all | bytes 8388608 | tf_op jit(solution)/shard_map/all_to_all | solution.py:41
  197.3 3.5 %reduce_sum.94 = bf16[4,128,2048]{2,1,0:T(8,128)(2,1)S(1)} reduce(bf16[2,4,128,2048]{3,2,1,0:T(8,128)(2,1)} %all_to_all.51, bf16[]{:T(256)} %constant.43.clone.1), dimensions={0}, to_apply=%region_7.8 | reduce | flops 1048576 | bytes 6291458 | tf_op jit(solution)/shard_map/reduce_sum | solution.py:42
  200.8 0.0 copy-start.1
  200.9 29.4 %all_to_all.52 = bf16[4,128,2048]{2,1,0:T(8,128)(2,1)S(1)} all-to-all(bf16[4,128,2048]{2,1,0:T(8,128)(2,1)S(1)} %reduce_sum.94), channel_id=1, replica_groups=mesh['fs'=16,'tp_0'=4,'tp_1'=2] {'tp_0'}, dimensions={0} | all-to-all | bytes 4194304 | tf_op jit(solution)/shard_map/all_to_all | solution.py:49
  230.2 0.4 convert_reduce_fusion
  230.6 0.9 fusion.40
  (19 shorter events, 0.1 us)
Async XLA Ops:
  6.5 39.3 %copy-start = (f32[8,128]{1,0:T(8,128)S(1)}, f32[8,128]{1,0:T(8,128)}, u32[]{:S(2)}) copy-start(f32[8,128]{1,0:T(8,128)} %param.27) | copy-start | bytes 12292
  6.5 8.0 %copy-start.2 = (bf16[128,2048]{1,0:T(8,128)(2,1)S(1)}, bf16[128,2048]{1,0:T(8,128)(2,1)}, u32[]{:S(2)}) copy-start(bf16[128,2048]{1,0:T(8,128)(2,1)} %param.18) | copy-start | bytes 1572868
  6.5 8.2 %copy-start.3 = (f32[2048]{0:T(1024)S(1)}, f32[2048]{0:T(1024)}, u32[]{:S(2)}) copy-start(f32[2048]{0:T(1024)} %param.19) | copy-start | bytes 24580
  6.5 58.3 %all-gather.3.cloned.1.call-start = ((), (), s32[]{:S(2)}) async-start(), calls=%async_computation.9 | async-start | bytes 3342336 | tf_op jit(solution)/shard_map/all_gather | solution.py:56
  10.3 154.7 %all-gather.5.cloned.1.call-start = ((), (), s32[]{:S(2)}) async-start(), calls=%async_computation.10 | async-start | bytes 10027008 | tf_op jit(solution)/shard_map/all_gather | solution.py:56
  15.0 6.2 %copy-start.6 = (f32[128]{0:T(128)S(1)}, f32[128]{0:T(128)}, u32[]{:S(2)}) copy-start(f32[128]{0:T(128)} %param.35) | copy-start | bytes 1540
  15.0 6.2 %copy-start.7 = (f32[128]{0:T(128)S(1)}, f32[128]{0:T(128)}, u32[]{:S(2)}) copy-start(f32[128]{0:T(128)} %param.29) | copy-start | bytes 1540
  16.6 30.9 %all-to-all-start = ((bf16[4,128,2048]{2,1,0:T(8,128)(2,1)}), bf16[4,128,2048]{2,1,0:T(8,128)(2,1)S(1)}, u32[]{:S(2)}, u32[]{:S(2)}) async-start(bf16[4,128,2048]{2,1,0:T(8,128)(2,1)} %broadcast_in_dim.13), calls=%async_computation | async-start | bytes 4194304 | tf_op jit(solution)/shard_map/all_to_all | solution.py:16
  55.1 9.8 %copy-start.10 = (f32[256]{0:T(256)S(1)}, f32[256]{0:T(256)}, u32[]{:S(2)}) copy-start(f32[256]{0:T(256)} %param.24) | copy-start | bytes 3076
  64.9 9.1 %copy-start.11 = (f32[256]{0:T(256)S(1)}, f32[256]{0:T(256)}, u32[]{:S(2)}) copy-start(f32[256]{0:T(256)} %param.22) | copy-start | bytes 3076
  69.7 9.9 %all-to-all-start.2 = ((f32[8,1,2048]{2,1,0:T(1,128)}), f32[8,1,2048]{2,1,0:T(1,128)S(1)}, u32[]{:S(2)}, u32[]{:S(2)}) async-start(f32[8,1,2048]{2,1,0:T(1,128)} %broadcast_in_dim.15), calls=%async_computation.2 | async-start | bytes 131072 | tf_op jit(solution)/shard_map/all_to_all | solution.py:16
  74.0 5.7 %copy-start.5 = (f32[256]{0:T(256)S(1)}, f32[256]{0:T(256)}, u32[]{:S(2)}) copy-start(f32[256]{0:T(256)} %param.25) | copy-start | bytes 3076
  125.9 0.7 copy-start.4
  165.0 8.2 %copy-start.8 = (f32[768]{0:T(1024)S(1)}, f32[768]{0:T(1024)}, u32[]{:S(2)}) copy-start(f32[768]{0:T(1024)} %param.33) | copy-start | bytes 9220
  165.0 8.2 %copy-start.9 = (f32[768]{0:T(1024)S(1)}, f32[768]{0:T(1024)}, u32[]{:S(2)}) copy-start(f32[768]{0:T(1024)} %param.31) | copy-start | bytes 9220
  200.8 30.7 %copy-start.1 = (f32[8,128]{1,0:T(8,128)S(1)}, f32[8,128]{1,0:T(8,128)}, u32[]{:S(2)}) copy-start(f32[8,128]{1,0:T(8,128)} %param.27) | copy-start | bytes 12292
Sparse Core Ops, SparseCore 0:
  10.4 54.4 all-gather.2
  67.0 81.8 all-gather.4
where the time goes:
time: 240 us; the launch traced here: 238 us
  blocking collectives  143 us (60%)
  matrix products  33.5 us (14%)
  local copies, waits for them, and re-layouts  15.9 us (7%)
  between operations  13.6 us (6%)
  other arithmetic  13.5 us (6%)
  waiting for transfers between devices  10.4 us (4%)
  starting transfers between devices  8.9 us (4%)
    all_to_all x2, blocking collectives, sum_in_two_steps(): lax.all_to_all(own.astype(jnp.bfloat16), far, 0, 0, tiled=True)  59.4 us
    all_to_all x3, blocking collectives, copy_for_each(): lax.all_to_all(jnp.broadcast_to(value[None], (peers, *value.shape)), axis...  42.2 us
    all_gather x1, blocking collectives, turned_gather(): out, at, finished = (lax.all_gather(both, axis, axis=0, tiled=True), 0, [])  24.7 us
    all_to_all x2, blocking collectives, sent_and_summed(): lax.all_to_all(tiles, axis, split_axis=0, concat_axis=0, tiled=True)  16.3 us
    dot_general x1, matrix products, ffn_term(): jnp.dot(hidden, down_whole, preferred_element_type=jnp.float32)  13.4 us
    all_to_all x2, starting transfers between devices, copy_for_each(): lax.all_to_all(jnp.broadcast_to(value[None], (peers, *value.shape)), axis...  8.86 us
    dot_general x1, matrix products, project_ffn(): jnp.dot(segment, up_whole, preferred_element_type=jnp.float32) * up_scale  8.24 us
    all_gather x2, waiting for transfers between devices, turned_gather(): out, at, finished = (lax.all_gather(both, axis, axis=0, tiled=True), 0, [])  7.4 us
  transfers between devices with their start and end apart: 4, of which 3 were waited for; matrix products, arithmetic and copies ran while one was open for 13% of the time, Pallas kernels for 0%

commit v1 on v0

v1 whole, which is shorter than its diff:
```python
import functools

import jax
import jax.numpy as jnp
from jax import lax
from jax.experimental import pallas as pl
from jax.experimental.pallas import tpu as pltpu
from jax.sharding import PartitionSpec as P

MESH = pl.DeviceIdType.MESH
F32 = jnp.float32
BF16 = jnp.bfloat16
A = 2048
BLK = 128
LEFT, RIGHT, OPP, OWN = 0, 1, 2, 3


def rms_rows(widened, norm_gain):
    factor = lax.rsqrt(jnp.mean(widened * widened, axis=1, keepdims=True) + 1e-06)
    return (widened * factor * norm_gain).astype(BF16)


def gelu(x):
    return 0.5 * x * (1.0 + jnp.tanh(0.7978845608028654 * (x + 0.044715 * (x * x * x))))


def silu(x):
    return 0.5 * x * (1.0 + jnp.tanh(0.5 * x))


class Sends:
    def __init__(self, sems):
        self.sems, self.started = sems, []

    def start(self, src, dst, recv_sem, device):
        copy = pltpu.make_async_remote_copy(
            src_ref=src,
            dst_ref=dst,
            send_sem=self.sems.at[len(self.started)],
            recv_sem=recv_sem,
            device_id=device,
            device_id_type=MESH,
        )
        copy.start()
        self.started.append(copy)

    def finish(self):
        for copy in self.started:
            copy.wait_send()


def arrived(ref, sem, device):
    pltpu.make_async_remote_copy(
        src_ref=ref,
        dst_ref=ref,
        send_sem=sem,
        recv_sem=sem,
        device_id=device,
        device_id_type=MESH,
    ).wait_recv()


class Gather:
    def __init__(self, buf, sems, sends, place, x_first):
        self.buf, self.sems, self.sends, self.place, self.x_first = buf, sems, sends, place, x_first

    def peer(self, first, step):
        pc = self.place
        along_x = first == self.x_first
        x = lax.rem(pc["x"] + step + 4, 4) if along_x else pc["x"]
        z = pc["z"] if along_x else lax.rem(pc["z"] + step + 4, 4)
        return (z * 4 + x, pc["y"] * 2 + pc["c"])

    def block(self, step, rows=None):
        pc = self.place
        x = lax.rem(pc["x"] + step + 4, 4) if self.x_first else pc["x"]
        z = pc["z"] if self.x_first else lax.rem(pc["z"] + step + 4, 4)
        ref = self.buf.at[pc["c"], z, x]
        return ref if rows is None else ref.at[rows]

    def group(self, step, half=None, core=None):
        pc = self.place
        core = pc["c"] if core is None else core
        part = slice(None) if half is None else pl.ds(2 * half, 2)
        if self.x_first:
            return self.buf.at[core, lax.rem(pc["z"] + step + 4, 4), part]
        return self.buf.at[core, part, lax.rem(pc["x"] + step + 4, 4)]

    def halves(self):
        rows = self.buf.shape[3] // 2
        return pl.ds(0, rows), pl.ds(rows, rows)

    def send(self, src, slot, device):
        self.sends.start(src, src, self.sems.at[slot], device)

    def share(self, ref, slot):
        self.send(ref, slot, self.place["partner"])

    def wait(self, ref, slot):
        arrived(ref, self.sems.at[slot], self.place["partner"])

    def first_start(self):
        self.send(self.block(0), 0, self.peer(True, 1))
        self.send(self.block(0), 1, self.peer(True, -1))

    def first_relay(self):
        low, high = self.halves()
        self.wait(self.block(-1), 0)
        self.send(self.block(-1, low), 2, self.peer(True, 1))
        self.wait(self.block(1), 1)
        self.send(self.block(1, high), 3, self.peer(True, -1))

    def second_start(self):
        low, high = self.halves()
        self.wait(self.block(2, low), 2)
        self.wait(self.block(2, high), 3)
        self.send(self.group(0), 4, self.peer(False, 1))
        self.send(self.group(0), 5, self.peer(False, -1))
        self.share(self.group(0), 8)

    def second_relay(self):
        self.wait(self.group(-1), 4)
        self.send(self.group(-1, 0), 6, self.peer(False, 1))
        self.share(self.group(-1), 9)
        self.wait(self.group(1), 5)
        self.send(self.group(1, 1), 7, self.peer(False, -1))
        self.share(self.group(1), 10)

    def second_end(self):
        self.wait(self.group(2, 0), 6)
        self.share(self.group(2, 0), 11)
        self.wait(self.group(2, 1), 7)
        self.share(self.group(2, 1), 12)

    def from_partner(self):
        other = 1 - self.place["c"]
        self.wait(self.group(0, core=other), 8)
        self.wait(self.group(-1, core=other), 9)
        self.wait(self.group(1, core=other), 10)
        self.wait(self.group(2, 0, other), 11)
        self.wait(self.group(2, 1, other), 12)


N_GATHER_SEMS = 13
N_SENDS = 160


def layer_kernel(
    tok_hbm, u_hbm, v_hbm, o_hbm, g_hbm, p_hbm, d_hbm,
    mix_gain, ffn_gain, u_scale, v_scale, v_gain, o_scale, g_scale, p_scale, d_scale,
    spatial, bias, out_ref,
    tok, u32, v32, o32, g32, p32, d32,
    ub, vb, oab, obb, gb, pb, dab, dbb,
    x1, x2, u_val, v_val, gated, hid, part1, part2, relay1, relay2, fl1, fr1, fl2, fr2, res,
    stat, stat_in, vg,
    load_sems, send_sems, gather_sems, tok_sems, misc_sems,
):
    fs = lax.axis_index("fs")
    tp = lax.axis_index("tp")
    z, x = fs // 4, lax.rem(fs, 4)
    y, c = tp // 2, lax.rem(tp, 2)
    partner = (fs, y * 2 + (1 - c))
    y_right = (fs, lax.rem(y + 1, 4) * 2 + c)
    y_left = (fs, lax.rem(y + 3, 4) * 2 + c)
    y_opp = (fs, lax.rem(y + 2, 4) * 2 + c)
    place = {"x": x, "y": y, "z": z, "c": c, "partner": partner}

    loads = []
    for n, (src, dst) in enumerate(
        ((tok_hbm, tok), (u_hbm, u32), (v_hbm, v32), (o_hbm, o32), (g_hbm, g32), (p_hbm, p32), (d_hbm, d32))
    ):
        copy = pltpu.make_async_copy(src, dst, load_sems.at[n])
        copy.start()
        loads.append(copy)

    barrier = pltpu.get_barrier_semaphore()
    plane = [
        (z * 4 + lax.rem(x + 1, 4), tp),
        (z * 4 + lax.rem(x + 3, 4), tp),
        (lax.rem(z + 1, 4) * 4 + x, tp),
        (lax.rem(z + 3, 4) * 4 + x, tp),
    ]
    peers = [partner, y_right, y_left, y_opp] + plane
    for peer in peers:
        pl.semaphore_signal(barrier, inc=1, device_id=peer, device_id_type=MESH)

    sends = Sends(send_sems)
    gather = [
        Gather(buf, gather_sems.at[n], sends, place, n % 2 == 0)
        for n, buf in enumerate((ub, vb, oab, obb, gb, pb, dab, dbb))
    ]
    gu, gv, goa, gob, gg, gp, gda, gdb = gather
    uv, outs, ffn, downs = (gu, gv), (goa, gob), (gg, gp), (gda, gdb)

    loads[1].wait()
    ub[c, z, x] = (u32[...] * u_scale[...]).astype(BF16)
    loads[2].wait()
    vb[c, z, x] = (v32[...] * v_scale[...]).astype(BF16)
    loads[3].wait()
    half = o32.shape[0] // 2
    oab[c, z, x] = (o32[:half] * o_scale[...]).astype(BF16)
    obb[c, z, x] = (o32[half:] * o_scale[...]).astype(BF16)
    vg[c] = jnp.broadcast_to(v_gain[...], vg.shape[1:])
    loads[0].wait()
    x1[OWN] = rms_rows(tok[...].astype(F32), mix_gain[...])

    pl.semaphore_wait(barrier, len(peers))

    H0, H1 = pl.ds(0, 64), pl.ds(64, 64)

    def rows_start(buf, base):
        sends.start(buf.at[OWN, H0], buf.at[LEFT, H0], tok_sems.at[base + 0], y_right)
        sends.start(buf.at[OWN, H1], buf.at[RIGHT, H1], tok_sems.at[base + 1], y_left)
        sends.start(buf.at[OWN, H1], buf.at[LEFT, H1], tok_sems.at[base + 2], y_right)
        sends.start(buf.at[OWN, H0], buf.at[RIGHT, H0], tok_sems.at[base + 3], y_left)

    def rows_relay(buf, base):
        arrived(buf.at[LEFT, H0], tok_sems.at[base + 0], y_left)
        sends.start(buf.at[LEFT, H0], buf.at[OPP, H0], tok_sems.at[base + 4], y_right)
        arrived(buf.at[RIGHT, H1], tok_sems.at[base + 1], y_right)
        sends.start(buf.at[RIGHT, H1], buf.at[OPP, H1], tok_sems.at[base + 5], y_left)

    def rows_near(buf, base):
        arrived(buf.at[LEFT, H1], tok_sems.at[base + 2], y_left)
        arrived(buf.at[RIGHT, H0], tok_sems.at[base + 3], y_right)

    def rows_far(buf, base):
        arrived(buf.at[OPP, H0], tok_sems.at[base + 4], y_left)
        arrived(buf.at[OPP, H1], tok_sems.at[base + 5], y_right)

    def sums_far(part, relay, base):
        sends.start(part.at[OPP, H0], relay.at[0], tok_sems.at[base + 0], y_right)
        sends.start(part.at[OPP, H1], relay.at[1], tok_sems.at[base + 1], y_left)

    def sums_near(part, fl, fr, base):
        sends.start(part.at[RIGHT, H1], fl.at[H1], tok_sems.at[base + 2], y_right)
        sends.start(part.at[LEFT, H0], fr.at[H0], tok_sems.at[base + 3], y_left)

    def sums_relay(part, relay, fl, fr, base):
        arrived(relay.at[0], tok_sems.at[base + 0], y_left)
        part[RIGHT, H0] = (part[RIGHT, H0].astype(F32) + relay[0].astype(F32)).astype(BF16)
        sends.start(part.at[RIGHT, H0], fl.at[H0], tok_sems.at[base + 4], y_right)
        arrived(relay.at[1], tok_sems.at[base + 1], y_right)
        part[LEFT, H1] = (part[LEFT, H1].astype(F32) + relay[1].astype(F32)).astype(BF16)
        sends.start(part.at[LEFT, H1], fr.at[H1], tok_sems.at[base + 5], y_left)

    def sums_end(fl, fr, base):
        arrived(fl.at[H1], tok_sems.at[base + 2], y_left)
        arrived(fr.at[H0], tok_sems.at[base + 3], y_right)
        arrived(fl.at[H0], tok_sems.at[base + 4], y_left)
        arrived(fr.at[H1], tok_sems.at[base + 5], y_right)

    for g in uv:
        g.first_start()
    rows_start(x1, 0)
    for g in outs:
        g.first_start()
    sends.start(vg.at[c], vg.at[c], misc_sems.at[3], partner)

    loads[4].wait()
    gb[c, z, x] = (g32[...] * g_scale[...]).astype(BF16)
    loads[5].wait()
    pb[c, z, x] = (p32[...] * p_scale[...]).astype(BF16)
    loads[6].wait()
    half = d32.shape[0] // 2
    dab[c, z, x] = (d32[:half] * d_scale[...]).astype(BF16)
    dbb[c, z, x] = (d32[half:] * d_scale[...]).astype(BF16)

    for g in uv:
        g.first_relay()
    for g in outs:
        g.first_relay()
    for g in uv:
        g.second_start()
    rows_relay(x1, 0)
    for g in uv:
        g.second_relay()
    for g in outs:
        g.second_start()
    for g in ffn:
        g.first_start()
    for g in uv:
        g.second_end()
    rows_near(x1, 0)
    rows_far(x1, 0)
    for g in outs:
        g.second_relay()
    for g in uv:
        g.from_partner()

    slot_chip = [lax.rem(y + 3, 4), lax.rem(y + 1, 4), lax.rem(y + 2, 4), y]
    row_ids = lax.broadcasted_iota(jnp.int32, (BLK, BLK), 0)
    col_ids = lax.broadcasted_iota(jnp.int32, (BLK, BLK), 1)
    eye = row_ids == col_ids
    stat[...] = jnp.zeros_like(stat)

    def project_mixer(first):
        rows = x1[first : first + 2].reshape(2 * BLK, -1)
        sums = squares = None
        for core in range(2):
            cols = slice(core * 256, core * 256 + 256)
            u = gelu(jnp.dot(rows, ub[core].reshape(A, 256), preferred_element_type=F32))
            v = gelu(jnp.dot(rows, vb[core].reshape(A, 256), preferred_element_type=F32)).astype(BF16)
            u_val[first : first + 2, :, cols] = u.astype(BF16).reshape(2, BLK, 256)
            v_val[first : first + 2, :, cols] = v.reshape(2, BLK, 256)
            wide = v.astype(F32)
            s, q = jnp.sum(wide, axis=1, keepdims=True), jnp.sum(wide * wide, axis=1, keepdims=True)
            sums, squares = (s, q) if core == 0 else (sums + s, squares + q)
        for k in range(2):
            for row, column in ((0, sums), (1, squares)):
                piece = column[k * BLK : (k + 1) * BLK]
                stat[slot_chip[first + k], row : row + 1, :] = jnp.sum(
                    jnp.where(eye, piece, 0.0), axis=0, keepdims=True
                )

    project_mixer(LEFT)
    for g in ffn:
        g.first_relay()
    project_mixer(OPP)
    sends.start(stat, stat_in.at[0], misc_sems.at[0], y_right)
    sends.start(stat, stat_in.at[1], misc_sems.at[1], y_left)
    sends.start(stat, stat_in.at[2], misc_sems.at[2], y_opp)
    for g in outs:
        g.second_end()
    for g in ffn:
        g.second_start()
    for g in downs:
        g.first_start()
    arrived(vg.at[1 - c], misc_sems.at[3], partner)
    arrived(stat_in.at[0], misc_sems.at[0], y_left)
    arrived(stat_in.at[1], misc_sems.at[1], y_right)
    arrived(stat_in.at[2], misc_sems.at[2], y_opp)

    mixers = []
    for core in range(2):
        masked = jnp.where(col_ids <= row_ids, spatial[2 * y + core].astype(F32), 0.0)
        offset = jnp.sum(jnp.where(eye, bias[2 * y + core], 0.0), axis=1, keepdims=True)
        mixers.append((masked, offset))

    def mix(slot):
        chip = slot_chip[slot]
        total = stat[chip] + stat_in[0, chip] + stat_in[1, chip] + stat_in[2, chip]
        average = total[0:1] * (1.0 / A)
        spread = total[1:2] * (1.0 / A) - average * average
        factor = lax.rsqrt(spread + 1e-05)
        for core in range(2):
            cols = slice(core * 256, core * 256 + 256)
            masked, offset = mixers[core]
            scaled = (masked * factor).astype(BF16)
            shift = jnp.sum(scaled.astype(F32) * average, axis=1, keepdims=True)
            mixed = jnp.dot(scaled, v_val[slot, :, cols], preferred_element_type=F32)
            mixed = (mixed - shift) * vg[core, 0:1, :] + offset
            gated[slot, :, cols] = (u_val[slot, :, cols].astype(F32) * mixed).astype(BF16)

    def project_out(first):
        @pl.loop(0, 8)
        def _(j):
            fz, fx = j // 2, lax.rem(j, 2) * 2
            total = None
            for core in range(2):
                matrix = jnp.concatenate(
                    [
                        jnp.concatenate([oab[core, fz, fx], obb[core, fz, fx]], axis=0),
                        jnp.concatenate([oab[core, fz, fx + 1], obb[core, fz, fx + 1]], axis=0),
                    ],
                    axis=1,
                )
                rows = gated[first : first + 2, :, core * 256 : core * 256 + 256].reshape(2 * BLK, 256)
                term = jnp.dot(rows, matrix, preferred_element_type=F32)
                total = term if core == 0 else total + term
            cols = pl.ds(pl.multiple_of(j * 256, 256), 256)
            part1[first : first + 2, :, cols] = total.astype(BF16).reshape(2, BLK, 256)

    mix(OPP)
    mix(OWN)
    for g in outs:
        g.from_partner()
    project_out(OPP)
    sums_far(part1, relay1, 6)
    mix(LEFT)
    mix(RIGHT)
    project_out(LEFT)
    sums_near(part1, fl1, fr1, 6)
    sums_relay(part1, relay1, fl1, fr1, 6)
    for g in downs:
        g.first_relay()
    sums_end(fl1, fr1, 6)
    total = tok[...].astype(F32) + part1[OWN].astype(F32)
    residual = (total + fl1[...].astype(F32) + fr1[...].astype(F32)).astype(BF16)
    res[...] = residual
    x2[OWN] = rms_rows(residual.astype(F32), ffn_gain[...])
    rows_start(x2, 12)
    for g in ffn:
        g.second_relay()
    rows_relay(x2, 12)
    for g in downs:
        g.second_start()
    for g in ffn:
        g.second_end()
    rows_near(x2, 12)
    for g in ffn:
        g.from_partner()

    def project_ffn(first):
        @pl.loop(0, 2)
        def _(core):
            for j in range(3):
                cols = slice(j * 256, j * 256 + 256)
                rows = x2[first : first + 2].reshape(2 * BLK, -1)
                gate = jnp.dot(rows, gb[core, :, :, :, cols].reshape(A, 256), preferred_element_type=F32)
                up = jnp.dot(rows, pb[core, :, :, :, cols].reshape(A, 256), preferred_element_type=F32)
                hid[core, :, cols] = (silu(gate) * up).astype(BF16)

    def project_down(first):
        @pl.loop(0, 8)
        def _(j):
            fz, fx = j // 2, lax.rem(j, 2) * 2
            total = None
            for core in range(2):
                matrix = jnp.concatenate(
                    [
                        jnp.concatenate([dab[core, fz, fx], dbb[core, fz, fx]], axis=0),
                        jnp.concatenate([dab[core, fz, fx + 1], dbb[core, fz, fx + 1]], axis=0),
                    ],
                    axis=1,
                )
                term = jnp.dot(hid[core], matrix, preferred_element_type=F32)
                total = term if core == 0 else total + term
            cols = pl.ds(pl.multiple_of(j * 256, 256), 256)
            part2[first : first + 2, :, cols] = total.astype(BF16).reshape(2, BLK, 256)

    project_ffn(LEFT)
    for g in downs:
        g.second_relay()
    for g in downs:
        g.second_end()
    for g in downs:
        g.from_partner()
    project_down(LEFT)
    sums_near(part2, fl2, fr2, 18)
    rows_far(x2, 12)
    project_ffn(OPP)
    project_down(OPP)
    sums_far(part2, relay2, 18)
    sums_relay(part2, relay2, fl2, fr2, 18)
    sums_end(fl2, fr2, 18)
    total = res[...].astype(F32) + part2[OWN].astype(F32)
    out_ref[...] = (total + fl2[...].astype(F32) + fr2[...].astype(F32)).astype(BF16)
    sends.finish()


def local(
    tokens, mix_gain, ffn_gain, u_weight, u_scale, v_weight, v_scale, v_gain, spatial_weight, spatial_bias,
    out_weight, out_scale, gate_weight, gate_scale, up_weight, up_scale, down_weight, down_scale,
):
    rows, width = tokens.shape
    row = lambda a: a.reshape(1, -1)
    bias = spatial_bias.reshape(spatial_bias.shape[0], 1, BLK)
    depth = u_weight.shape[0]
    ff = gate_weight.shape[1]
    mix_cols = u_weight.shape[1]
    out_cols = out_weight.shape[1]
    vm = pltpu.VMEM
    anywhere = pl.BlockSpec(memory_space=pl.ANY)
    on_chip = pl.BlockSpec(memory_space=pltpu.VMEM)
    scratch = [
        vm(tokens.shape, BF16),
        vm(u_weight.shape, F32), vm(v_weight.shape, F32), vm(out_weight.shape, F32),
        vm(gate_weight.shape, F32), vm(up_weight.shape, F32), vm(down_weight.shape, F32),
        vm((2, 4, 4, depth, mix_cols), BF16), vm((2, 4, 4, depth, mix_cols), BF16),
        vm((2, 4, 4, mix_cols // 2, out_cols), BF16), vm((2, 4, 4, mix_cols // 2, out_cols), BF16),
        vm((2, 4, 4, depth, ff), BF16), vm((2, 4, 4, depth, ff), BF16),
        vm((2, 4, 4, ff // 2, out_cols), BF16), vm((2, 4, 4, ff // 2, out_cols), BF16),
        vm((4, rows, width), BF16), vm((4, rows, width), BF16),
        vm((4, rows, 2 * mix_cols), BF16), vm((4, rows, 2 * mix_cols), BF16), vm((4, rows, 2 * mix_cols), BF16),
        vm((2, 2 * rows, ff), BF16),
        vm((4, rows, width), BF16), vm((4, rows, width), BF16),
        vm((2, rows // 2, width), BF16), vm((2, rows // 2, width), BF16),
        vm((rows, width), BF16), vm((rows, width), BF16), vm((rows, width), BF16), vm((rows, width), BF16),
        vm((rows, width), BF16),
        vm((4, 8, BLK), F32), vm((3, 4, 8, BLK), F32), vm((2, 8, mix_cols), F32),
        pltpu.SemaphoreType.DMA((7,)),
        pltpu.SemaphoreType.DMA((N_SENDS,)),
        pltpu.SemaphoreType.DMA((8, N_GATHER_SEMS)),
        pltpu.SemaphoreType.DMA((24,)),
        pltpu.SemaphoreType.DMA((4,)),
    ]
    return pl.pallas_call(
        layer_kernel,
        out_shape=jax.ShapeDtypeStruct(tokens.shape, BF16),
        in_specs=[anywhere] * 7 + [on_chip] * 11,
        out_specs=on_chip,
        scratch_shapes=scratch,
        compiler_params=pltpu.CompilerParams(
            collective_id=0, has_side_effects=True, vmem_limit_bytes=60 * 1024 * 1024
        ),
    )(
        tokens, u_weight, v_weight, out_weight, gate_weight, up_weight, down_weight,
        row(mix_gain), row(ffn_gain), row(u_scale), row(v_scale), row(v_gain), row(out_scale),
        row(gate_scale), row(up_scale), row(down_scale), spatial_weight, bias,
    )


def solution(mesh):
    both = ("fs", "tp")
    in_specs = (
        P(both, None), P(), P(),
        P("fs", "tp"), P("tp"), P("fs", "tp"), P("tp"), P("tp"),
        P(), P(),
        P("tp", "fs"), P("fs"),
        P("fs", "tp"), P("tp"), P("fs", "tp"), P("tp"),
        P("tp", "fs"), P("fs"),
    )
    return jax.shard_map(local, mesh=mesh, in_specs=in_specs, out_specs=P(both, None), check_vma=False)
```

time: 240 us -> 118 us (0.49)
  blocking collectives: 143 us -> 0 us
  Pallas kernels: 0 us -> 114 us
  matrix products: 33.5 us -> 0 us
  between operations: 13.6 us -> 0.01 us
  other arithmetic: 13.5 us -> 0 us
  local copies, waits for them, and re-layouts: 15.9 us -> 3.75 us
  waiting for transfers between devices: 10.4 us -> 0 us
  starting transfers between devices: 8.9 us -> 0 us
    all_to_all x7 -> x0, blocking collectives: 118 us -> none  [the longest x2 59.4 us: sum_in_two_steps(): lax.all_to_all(own.astype(jnp.bfloat16), far, 0, 0, tiled=True)]
    pallas_call x0 -> x1, Pallas kernels: none -> 114 us  [local(): pl.pallas_call(layer_kernel, out_shape=jax.ShapeDtypeStruct(tokens.shape,...]
    dot_general x6 -> x0, matrix products: 33.5 us -> none  [the longest x1 13.4 us: ffn_term(): jnp.dot(hidden, down_whole, preferred_element_type=jnp.float32)]
    all_gather x1 -> x0, blocking collectives: 24.7 us -> none  [turned_gather(): out, at, finished = (lax.all_gather(both, axis, axis=0, tiled=True), 0, [])]
    all_to_all x2 -> x0, starting transfers between devices: 8.86 us -> none  [copy_for_each(): lax.all_to_all(jnp.broadcast_to(value[None], (peers, *value.shape)), axis...]
    reduce_sum x7 -> x0, other arithmetic: 8.36 us -> none  [the longest x2 7.11 us: sent_and_summed(): return arrived.astype(jnp.float32).sum(axis=0)]
    all_gather x2 -> x0, waiting for transfers between devices: 7.4 us -> none  [turned_gather(): out, at, finished = (lax.all_gather(both, axis, axis=0, tiled=True), 0, [])]
    all_to_all x2 -> x0, local copies, waits for them, and re-layouts: 4.76 us -> none  [copy_for_each(): lax.all_to_all(jnp.broadcast_to(value[None], (peers, *value.shape)), axis...]
  transfers between devices with their start and end apart: 4 -> 0, of which waited for: 3 -> 0; matrix products, arithmetic and copies ran while one was open for 13% -> 0% of each run, Pallas kernels for 0% -> 0%
where the time goes in v1:
time: 118 us; the launch traced here: 117 us
  Pallas kernels  114 us (97%)
  local copies, waits for them, and re-layouts  3.75 us (3%)
    pallas_call x1, Pallas kernels, local(): pl.pallas_call(layer_kernel, out_shape=jax.ShapeDtypeStruct(tokens.shape,...  114 us
    unnamed x5, local copies, waits for them, and re-layouts  2.57 us

profile of v1, /device:TPU:0, one launch (start us, length us, event | category | flops | bytes accessed | tf_op | source)
XLA Modules:
  0.0 117.3 jit_solution(14787743085478085439)
XLA Ops:
  0.0 0.0 copy-start
  0.0 0.0 copy-start.1
  0.0 0.7 copy-done
  0.7 0.6 reshape.36.g_scale
  1.3 0.0 copy-done.1
  1.3 0.6 reshape.37.p_scale
  1.9 113.6 %shard_map.172 = bf16[128,2048]{1,0:T(8,128)(2,1)} custom-call(bf16[128,2048]{1,0:T(8,128)(2,1)} %tok_hbm.1, f32[128,256]{1,0:T(8,128)} %u_hbm.1, f32[128,256]{1,0:T(8,128)} %v_hbm.1, f32[256,128]{1,0:T(8,128)} %o_hbm.1, f32[128,768]{1,0:T(8,128)} %g_hbm.1, f32[128,768]{1,0:T(8,128)} %p_hbm.1, f32[768,128]{1,0:T(8,128)} %d_hbm.1, f32[1,2048]{1,0:T(1,128)} %bitcast.8, ...), custom_call_target="tpu_custom_call" | custom-call | tf_op jit(solution)/shard_map/pallas_call | solution.py:488
  115.4 1.9 %copy.20 = bf16[128,2048]{1,0:T(8,128)(2,1)} copy(bf16[128,2048]{1,0:T(8,128)(2,1)} %shard_map.172) | data formatting | bytes 1048576
Async XLA Ops:
  0.0 0.7 copy-start
  0.0 1.3 %copy-start.1 = (f32[768]{0:T(1024)S(1)}, f32[768]{0:T(1024)}, u32[]{:S(2)}) copy-start(f32[768]{0:T(1024)} %param.33) | copy-start | bytes 9220

commit v2 on v0

v2 whole, which is shorter than its diff:
```python
import functools

import jax
import jax.numpy as jnp
from jax import lax
from jax.experimental import pallas as pl
from jax.experimental.pallas import tpu as pltpu
from jax.sharding import PartitionSpec as P

MESH = pl.DeviceIdType.MESH
F32 = jnp.float32
BF16 = jnp.bfloat16
A = 2048
BLK = 128
LEFT, RIGHT, OPP, OWN = 0, 1, 2, 3


def rms_rows(widened, norm_gain):
    factor = lax.rsqrt(jnp.mean(widened * widened, axis=1, keepdims=True) + 1e-06)
    return (widened * factor * norm_gain).astype(BF16)


def gelu(x):
    return 0.5 * x * (1.0 + jnp.tanh(0.7978845608028654 * (x + 0.044715 * (x * x * x))))


def silu(x):
    return 0.5 * x * (1.0 + jnp.tanh(0.5 * x))


ORDER = (
    184, 187, 185, 186, 235, 0, 1, 20, 21, 4, 5, 24,
    25, 2000, 136, 168, 1161, 44, 45, 64, 65, 40, 41, 60,
    61, 1000, 2, 6, 7, 1001, 3, 8, 9, 1012, 22, 26,
    27, 1013, 23, 28, 29, 1004, 12, 1016, 32, 1028, 1040, 1024,
    47, 1025, 43, 49, 1036, 67, 1037, 69, 1002, 42, 62, 63,
    52, 72, 1003, 16, 10, 11, 1110, 188, 1113, 189, 1006, 13,
    66, 1005, 1018, 33, 1017, 1008, 14, 1014, 68, 1015, 36, 30,
    31, 1020, 34, 1027, 1029, 46, 1041, 1032, 54, 48, 1026, 56,
    51, 1038, 1039, 76, 71, 1044, 74, 50, 70, 1009, 15, 18,
    1042, 73, 1111, 1112, 1007, 17, 1021, 35, 38, 1030, 53, 80,
    81, 100, 101, 1033, 58, 1045, 78, 1019, 37, 1010, 19, 1031,
    57, 1043, 77, 1022, 39, 55, 75, 104, 1114, 84, 85, 105,
    1115, 1011, 1023, 2001, 2002, 1048, 82, 1049, 1061, 2003, 83, 103,
    86, 1034, 59, 1046, 79, 1060, 2004, 233, 234, 232, 106, 1035,
    87, 107, 1047, 1064, 1159, 102, 1160, 1052, 1158, 2006, 2008, 204,
    205, 206, 207, 112, 2005, 2007, 202, 203, 92, 89, 109, 1050,
    1051, 96, 1063, 1054, 1066, 113, 1130, 93, 91, 1132, 2025, 208,
    1053, 1062, 116, 111, 1065, 2027, 210, 1131, 1133, 2026, 209, 2028,
    211, 108, 1056, 94, 88, 1068, 114, 110, 1128, 90, 1129, 1057,
    98, 95, 1069, 118, 115, 1134, 1136, 2037, 190, 191, 2039, 195,
    194, 120, 121, 152, 153, 1135, 1137, 2038, 192, 193, 2040, 197,
    196, 1067, 117, 124, 125, 156, 157, 1116, 198, 1117, 1055, 97,
    1058, 99, 1070, 119, 1072, 122, 140, 126, 127, 1073, 123, 144,
    1091, 172, 158, 1092, 176, 1120, 154, 155, 159, 1121, 200, 1095,
    169, 128, 129, 160, 1076, 137, 1077, 138, 1096, 170, 161, 1074,
    1118, 199, 1119, 1075, 148, 164, 1059, 130, 131, 1078, 141, 1079,
    142, 1097, 173, 1093, 1094, 180, 163, 1071, 1098, 174, 162, 133,
    1122, 1123, 201, 2009, 2010, 1099, 177, 1080, 145, 1081, 146, 134,
    2011, 132, 165, 1100, 178, 166, 2012, 1124, 1126, 2013, 1103, 171,
    1082, 149, 1083, 150, 135, 2014, 1102, 182, 167, 1088, 1107, 2021,
    212, 213, 1101, 181, 1085, 143, 1125, 1127, 2015, 1086, 147, 1090,
    2016, 1105, 179, 2017, 1104, 175, 1084, 139, 1109, 2018, 1087, 151,
    2019, 1106, 183, 2020, 2022, 214, 215, 216, 217, 1138, 1139, 1089,
    1108, 2024, 224, 225, 226, 227, 2023, 222, 223, 1140, 1142, 2029,
    218, 2031, 220, 1141, 1143, 2030, 219, 2032, 221, 1150, 1152, 2033,
    228, 2035, 230, 1151, 1153, 2034, 229, 2036, 231, 1148, 1149, 1144,
    1146, 1145, 1147, 2041, 1154, 1156, 1155, 1157, 2042,
)
N_FAMILIES, N_ARRIVALS = 31, 162


COLUMNS = (
    ((0, 0), (0, -1), (0, 1), (-1, 0), (1, 0), (-1, -1), (1, 1), (-1, 1)),
    ((1, -1), (2, 0), (0, 2), (2, 1), (1, 2), (2, -1), (-1, 2), (2, 2)),
)
OFFSETS = {"o": 0, "L": -1, "R": 1, "P": 2}


def weight_transfers(name, buf, x_first, place):
    x, y, z, c = place
    low, high = pl.ds(0, buf.shape[3] // 2), pl.ds(buf.shape[3] // 2, buf.shape[3] // 2)

    def at(value, step):
        return lax.rem(value + step + 4, 4)

    def block(a, b, rows=None):
        ref = buf.at[c, at(z, b), at(x, a)] if x_first else buf.at[c, at(z, a), at(x, b)]
        return ref if rows is None else ref.at[rows]

    def group(b, core=None):
        core = c if core is None else core
        return buf.at[core, at(z, b)] if x_first else buf.at[core, :, at(x, b)]

    def device(first, step):
        along_x = first == x_first
        return (z * 4 + at(x, step), y * 2 + c) if along_x else (at(z, step) * 4 + x, y * 2 + c)

    found = {}
    for sign, step in (("+", 1), ("-", -1)):
        rows = low if step == 1 else high
        found["1" + sign] = (block(0, 0), device(True, step), block(-step, 0))
        found["1f" + sign] = (block(-step, 0, rows), device(True, step), block(2, 0, rows))
        far = device(False, step)
        for kind, a in OFFSETS.items():
            found["2" + kind + sign] = (block(a, 0), far, block(a, -step))
            found["2f" + kind + sign] = (block(a, -step), far, block(a, 2))
    partner = (z * 4 + x, y * 2 + 1 - c)
    parts = {"d0": 0, "d-": -1, "d+": 1, "d2": 2}
    for kind, a in OFFSETS.items():
        for mark, b in (("o", 0), ("-", -1), ("+", 1), ("2", 2)):
            other = buf.at[1 - c, at(z, b), at(x, a)] if x_first else buf.at[1 - c, at(z, a), at(x, b)]
            found["e" + kind + mark] = (block(a, b), partner, other)
    for key, b in parts.items():
        found[key] = (group(b), partner, group(b, core=1 - c))
    shared = list(parts) if name[0] != "D" else ["e" + kind + mark for kind in OFFSETS for mark in "o-+2"]
    used = ["1+", "1-", "1f+", "1f-"] + ["2" + kind + sign for kind in OFFSETS for sign in "+-"]
    used += ["2fo+", "2fL+", "2fR-", "2fP-"] + shared
    return {name + ":" + key: (found[key][0],) + found[key] for key in used}


def arrival_group(name):
    head, _, key = name.partition(":")
    if key[0] == "e":
        early = key[1] != "P" and key[2] != "2"
        return (head, "ea", 9) if early else (head, "eb", 4) if key[2] == "2" else (head, "ec", 3)
    if head[0] != "D":
        if key[0] == "d":
            return head, "d", 16
        if key[:2] == "2f":
            return head, "2f", 4
        if key in ("2R+", "2P+"):
            return head, "2a", 2
        if key in ("2o-", "2L-"):
            return head, "2b", 2
    return head, key, 1


def layer_kernel(
    *refs,
):
    held_in_hbm, out_ref, held, refs = refs[:18], refs[18], refs[19:37], refs[37:]
    tok, mix_gain, u32, u_scale, v32, v_scale, o32, o_scale, v_gain, g32, g_scale, p32, p_scale, d32, d_scale, *rest = held
    spatial, bias, ffn_gain = rest
    (
        ub, vb, oab, obb, gb, pb, dab, dbb,
        x1, x2, u_val, v_val, gated, hid, part1, part2, relay1, relay2, fl1, fr1, fl2, fr2, res,
        stat, stat_in, vg,
        load_sems, send_sems, recv_sems,
    ) = refs
    fs = lax.axis_index("fs")
    tp = lax.axis_index("tp")
    z, x = fs // 4, lax.rem(fs, 4)
    y, c = tp // 2, lax.rem(tp, 2)
    partner = (fs, y * 2 + 1 - c)
    y_right = (fs, lax.rem(y + 1, 4) * 2 + c)
    y_left = (fs, lax.rem(y + 3, 4) * 2 + c)
    y_opp = (fs, lax.rem(y + 2, 4) * 2 + c)

    loads = []
    for n, (src, dst) in enumerate(zip(held_in_hbm, held)):
        copy = pltpu.make_async_copy(src, dst, load_sems.at[n])
        copy.start()
        loads.append((n, copy))

    barrier = pltpu.get_barrier_semaphore()
    plane = [
        (z * 4 + lax.rem(x + 1, 4), tp),
        (z * 4 + lax.rem(x + 3, 4), tp),
        (lax.rem(z + 1, 4) * 4 + x, tp),
        (lax.rem(z + 3, 4) * 4 + x, tp),
    ]
    peers = [partner, y_right, y_left, y_opp] + plane
    for peer in peers:
        pl.semaphore_signal(barrier, inc=1, device_id=peer, device_id_type=MESH)

    def ready(last):
        while loads[0][0] <= last:
            loads.pop(0)[1].wait()
            if not loads:
                break

    ready(3 + 2)
    ub[c, z, x] = (u32[...] * u_scale[...]).astype(BF16)
    vb[c, z, x] = (v32[...] * v_scale[...]).astype(BF16)
    x1[OWN] = rms_rows(tok[...].astype(F32), mix_gain[...])
    ready(8)
    half = o32.shape[0] // 2
    oab[c, z, x] = (o32[:half] * o_scale[...]).astype(BF16)
    obb[c, z, x] = (o32[half:] * o_scale[...]).astype(BF16)
    vg[c] = jnp.broadcast_to(v_gain[...], vg.shape[1:])

    pl.semaphore_wait(barrier, len(peers))


    moves = {}
    for n, (name, buf) in enumerate(
        (("U", ub), ("V", vb), ("OA", oab), ("OB", obb), ("G", gb), ("Q", pb), ("DA", dab), ("DB", dbb))
    ):
        moves.update(weight_transfers(name, buf, n % 2 == 0, (x, y, z, c)))

    H0, H1 = pl.ds(0, 64), pl.ds(64, 64)
    Q = [pl.ds(32 * q, 32) for q in range(4)]

    def rows_move(buf, to_right, rows):
        to = LEFT if to_right else RIGHT
        return (buf.at[OWN, rows], buf.at[to, rows], y_right if to_right else y_left, buf.at[to, rows])

    def pass_on(buf, to_right, rows):
        kept = LEFT if to_right else RIGHT
        return (buf.at[kept, rows], buf.at[OPP, rows], y_right if to_right else y_left, buf.at[OPP, rows])

    moves["X1:H0+"] = rows_move(x1, True, H0)
    moves["X1:H0-"] = rows_move(x1, False, H0)
    moves["X1:H1+"] = rows_move(x1, True, H1)
    moves["X1:H1-"] = rows_move(x1, False, H1)
    moves["X1:f+"] = pass_on(x1, True, H0)
    moves["X1:f-"] = pass_on(x1, False, H1)
    for q in range(4):
        moves[f"X2:{q}+"] = rows_move(x2, True, Q[q])
        moves[f"X2:{q}-"] = rows_move(x2, False, Q[q])
    for q in range(4):
        moves[f"X2:f{q}"] = pass_on(x2, q < 2, Q[q])
    for key, part, relay, fl, fr in (
        ("S1", part1, relay1, fl1, fr1),
        ("S2", part2.at[0], relay2.at[0], fl2.at[0], fr2.at[0]),
        ("S3", part2.at[1], relay2.at[1], fl2.at[1], fr2.at[1]),
    ):
        moves[f"{key}:n+"] = (part.at[RIGHT, H1], fl.at[H1], y_right, fl.at[H1])
        moves[f"{key}:n-"] = (part.at[LEFT, H0], fr.at[H0], y_left, fr.at[H0])
        for q in range(4):
            to = y_right if q < 2 else y_left
            moves[f"{key}:o{q}"] = (part.at[OPP, Q[q]], relay.at[Q[q]], to, relay.at[Q[q]])
        for q in range(4):
            near, into, to = (RIGHT, fl, y_right) if q < 2 else (LEFT, fr, y_left)
            moves[f"{key}:r{q}"] = (part.at[near, Q[q]], into.at[Q[q]], to, into.at[Q[q]])
    moves["stat:R"] = (stat, stat_in.at[0], y_right, stat_in.at[0])
    moves["stat:L"] = (stat, stat_in.at[1], y_left, stat_in.at[1])
    moves["stat:P"] = (stat, stat_in.at[2], y_opp, stat_in.at[2])
    moves["vg"] = (vg.at[c], vg.at[c], partner, vg.at[1 - c])

    slot_chip = [lax.rem(y + 3, 4), lax.rem(y + 1, 4), lax.rem(y + 2, 4), y]
    row_ids = lax.broadcasted_iota(jnp.int32, (BLK, BLK), 0)
    col_ids = lax.broadcasted_iota(jnp.int32, (BLK, BLK), 1)
    eye = row_ids == col_ids

    def project_mixer(first, core):
        rows = x1[first : first + 2].reshape(2 * BLK, -1)
        cols = slice(core * 256, core * 256 + 256)
        u = gelu(jnp.dot(rows, ub[core].reshape(A, 256), preferred_element_type=F32))
        v = gelu(jnp.dot(rows, vb[core].reshape(A, 256), preferred_element_type=F32)).astype(BF16)
        u_val[first : first + 2, :, cols] = u.astype(BF16).reshape(2, BLK, 256)
        v_val[first : first + 2, :, cols] = v.reshape(2, BLK, 256)
        wide = v.astype(F32)
        columns = jnp.sum(wide, axis=1, keepdims=True), jnp.sum(wide * wide, axis=1, keepdims=True)
        for k in range(2):
            chip = slot_chip[first + k]
            for row in range(2):
                piece = columns[row][k * BLK : (k + 1) * BLK]
                turned = jnp.sum(jnp.where(eye, piece, 0.0), axis=0, keepdims=True)
                if core == 1:
                    turned = turned + stat[chip, row : row + 1, :]
                stat[chip, row : row + 1, :] = turned

    def mixing_rows(core):
        masked = jnp.where(col_ids <= row_ids, spatial[2 * y + core].astype(F32), 0.0)
        offset = jnp.sum(jnp.where(eye, bias[2 * y + core], 0.0), axis=1, keepdims=True)
        return masked, offset

    def mix(slot):
        chip = slot_chip[slot]
        total = stat[chip] + stat_in[0, chip] + stat_in[1, chip] + stat_in[2, chip]
        average = total[0:1] * (1.0 / A)
        spread = total[1:2] * (1.0 / A) - average * average
        factor = lax.rsqrt(spread + 1e-05)
        for core in range(2):
            cols = slice(core * 256, core * 256 + 256)
            masked, offset = mixing_rows(core)
            scaled = (masked * factor).astype(BF16)
            shift = jnp.sum(scaled.astype(F32) * average, axis=1, keepdims=True)
            mixed = jnp.dot(scaled, v_val[slot, :, cols], preferred_element_type=F32)
            mixed = (mixed - shift) * vg[core, 0:1, :] + offset
            gated[slot, :, cols] = (u_val[slot, :, cols].astype(F32) * mixed).astype(BF16)

    def project_out(first):
        rows = gated[first : first + 2].reshape(2 * BLK, -1)
        for j in range(8):
            fz, fx = j // 2, (j % 2) * 2
            matrix = jnp.concatenate(
                [
                    jnp.concatenate([buf[core, fz, fx + k] for core in range(2) for buf in (oab, obb)], axis=0)
                    for k in range(2)
                ],
                axis=1,
            )
            total = jnp.dot(rows, matrix, preferred_element_type=F32)
            part1[first : first + 2, :, j * 256 : j * 256 + 256] = total.astype(BF16).reshape(2, BLK, 256)

    def project_ffn(first, n):
        rows = x2[first : first + 2].reshape(2 * BLK, -1)
        core, j = n // 3, n % 3
        cols = slice(j * 256, j * 256 + 256)
        gate = jnp.dot(rows, gb[core, :, :, :, cols].reshape(A, 256), preferred_element_type=F32)
        up = jnp.dot(rows, pb[core, :, :, :, cols].reshape(A, 256), preferred_element_type=F32)
        hid[first // 2, :, n * 256 : n * 256 + 256] = (silu(gate) * up).astype(BF16)

    def place_of(dz, dx):
        return lax.rem(z + dz + 4, 4), lax.rem(x + dx + 4, 4)

    def project_down(first, part):
        rows = hid[first // 2]
        for j in range(0, 8, 2):
            pair = []
            for dz, dx in COLUMNS[part][j : j + 2]:
                fz, fx = place_of(dz, dx)
                pair.append(
                    jnp.concatenate([buf[core, fz, fx] for core in range(2) for buf in (dab, dbb)], axis=0)
                )
            total = jnp.dot(rows, jnp.concatenate(pair, axis=1), preferred_element_type=F32)
            cols = slice(j * BLK, j * BLK + 256)
            part2[part, first : first + 2, :, cols] = total.astype(BF16).reshape(2, BLK, 256)

    def add_relayed(part, relay, q):
        near = RIGHT if q < 2 else LEFT
        part[near, Q[q]] = (part[near, Q[q]].astype(F32) + relay[Q[q]].astype(F32)).astype(BF16)

    def second_norm(q):
        total = tok[Q[q]].astype(F32) + part1[OWN, Q[q]].astype(F32)
        residual = (total + fl1[Q[q]].astype(F32) + fr1[Q[q]].astype(F32)).astype(BF16)
        res[Q[q]] = residual
        x2[OWN, Q[q]] = rms_rows(residual.astype(F32), ffn_gain[...])

    def finish(part):
        for j, (dz, dx) in enumerate(COLUMNS[part]):
            fz, fx = place_of(dz, dx)
            cols = pl.ds(pl.multiple_of((fz * 4 + fx) * BLK, BLK), BLK)
            held = slice(j * BLK, j * BLK + BLK)
            total = res[:, cols].astype(F32) + part2[part, OWN, :, held].astype(F32)
            total = total + fl2[part, :, held].astype(F32) + fr2[part, :, held].astype(F32)
            out_ref[:, cols] = total

    def convert_rest():
        ready(14)
        gb[c, z, x] = (g32[...] * g_scale[...].reshape(1, -1)).astype(BF16)
        pb[c, z, x] = (p32[...] * p_scale[...].reshape(1, -1)).astype(BF16)
        half = d32.shape[0] // 2
        dab[c, z, x] = (d32[:half] * d_scale[...]).astype(BF16)
        dbb[c, z, x] = (d32[half:] * d_scale[...]).astype(BF16)
        stat[...] = jnp.zeros_like(stat)
        ready(17)

    halves = (LEFT, OPP)
    work = [convert_rest]
    work += [functools.partial(project_mixer, first, core) for first in halves for core in range(2)]
    work += [lambda: (mix(LEFT), mix(RIGHT)), lambda: (mix(OPP), mix(OWN))]
    work += [functools.partial(project_out, first) for first in halves]
    work += [functools.partial(project_ffn, first, n) for first in halves for n in range(6)]
    work += [functools.partial(project_down, first, part) for part in range(2) for first in halves]
    for part, relay in ((part1, relay1), (part2.at[0], relay2.at[0]), (part2.at[1], relay2.at[1])):
        work += [functools.partial(add_relayed, part, relay, q) for q in range(4)]
    work += [functools.partial(second_norm, q) for q in range(4)]
    work += [functools.partial(finish, part) for part in range(2)]

    families = {}
    for n, buf in (("U", ub), ("V", vb), ("OA", oab), ("OB", obb), ("G", gb), ("Q", pb), ("DA", dab), ("DB", dbb)):
        families[n + "1"] = buf.at[0, 0, pl.ds(0, 3)]
        families[n + "2"] = buf.at[0, pl.ds(0, 3)]
        families[n + "s"] = buf.at[0]
    families["X1"], families["X2"], families["S1"] = x1.at[pl.ds(0, 3)], x2.at[pl.ds(0, 3)], part1.at[pl.ds(0, 3)]
    families["S2"], families["S3"] = part2.at[0, pl.ds(0, 3)], part2.at[1, pl.ds(0, 3)]
    families["stat"], families["vg"] = stat_in, vg.at[0]
    family_sem = {name: n for n, name in enumerate(families)}

    def family_of(name):
        head, _, tail = name.partition(":")
        if head in families:
            return head
        return head + (tail[0] if tail[0] in "12" else "s")

    buffers = {"U": ub, "V": vb, "OA": oab, "OB": obb, "G": gb, "Q": pb, "DA": dab, "DB": dbb}
    arrivals, arrival_of = [], {}
    known = {}
    for name, (_, _, to, ref) in moves.items():
        head = name.partition(":")[0]
        key = name
        if head in buffers:
            key = arrival_group(name)
            buf, blocks = buffers[head], key[2]
            if blocks > 1:
                ref = {16: buf.at[0], 9: buf.at[0, pl.ds(0, 3), pl.ds(0, 3)]}.get(blocks)
                ref = buf.at[0, 0, pl.ds(0, blocks)] if ref is None else ref
        if key not in known:
            known[key] = len(arrivals)
            arrivals.append((ref, to))
        arrival_of[name] = known[key]
    names = list(moves)

    def start(n):
        name = names[n]
        src, dst, to, _ = moves[name]
        pltpu.make_async_remote_copy(
            src_ref=src, dst_ref=dst, send_sem=send_sems.at[family_sem[family_of(name)]],
            recv_sem=recv_sems.at[arrival_of[name]], device_id=to, device_id_type=MESH,
        ).start()

    def arrive(n):
        ref, to = arrivals[n]
        sem = recv_sems.at[n]
        pltpu.make_async_remote_copy(
            src_ref=ref, dst_ref=ref, send_sem=sem, recv_sem=sem, device_id=to, device_id_type=MESH
        ).wait_recv()

    acts = (start, arrive, lambda n: work[n]())
    for code in ORDER:
        step = functools.partial(acts[code // 1000], code % 1000)
        step()
    for name, ref in families.items():
        sem = send_sems.at[family_sem[name]]
        pltpu.make_async_remote_copy(
            src_ref=ref, dst_ref=ref, send_sem=sem, recv_sem=sem, device_id=partner, device_id_type=MESH
        ).wait_send()


def local(
    tokens, mix_gain, ffn_gain, u_weight, u_scale, v_weight, v_scale, v_gain, spatial_weight, spatial_bias,
    out_weight, out_scale, gate_weight, gate_scale, up_weight, up_scale, down_weight, down_scale,
):
    rows, width = tokens.shape
    row = lambda a: a.reshape(1, -1)
    bias = spatial_bias.reshape(spatial_bias.shape[0], 1, BLK)
    depth = u_weight.shape[0]
    ff = gate_weight.shape[1]
    mix_cols = u_weight.shape[1]
    out_cols = out_weight.shape[1]
    vm = pltpu.VMEM
    on_chip = pl.BlockSpec(memory_space=pltpu.VMEM)
    inputs = (
        tokens, row(mix_gain), u_weight, row(u_scale), v_weight, row(v_scale), out_weight, row(out_scale), row(v_gain),
        gate_weight, gate_scale, up_weight, up_scale, down_weight, row(down_scale), spatial_weight, bias, row(ffn_gain),
    )
    in_hbm = pl.BlockSpec(memory_space=pltpu.HBM)
    scratch = [vm(a.shape, a.dtype) for a in inputs] + [
        vm((2, 4, 4, depth, mix_cols), BF16), vm((2, 4, 4, depth, mix_cols), BF16),
        vm((2, 4, 4, mix_cols // 2, out_cols), BF16), vm((2, 4, 4, mix_cols // 2, out_cols), BF16),
        vm((2, 4, 4, depth, ff), BF16), vm((2, 4, 4, depth, ff), BF16),
        vm((2, 4, 4, ff // 2, out_cols), BF16), vm((2, 4, 4, ff // 2, out_cols), BF16),
        vm((4, rows, width), BF16), vm((4, rows, width), BF16),
        vm((4, rows, 2 * mix_cols), BF16), vm((4, rows, 2 * mix_cols), BF16), vm((4, rows, 2 * mix_cols), BF16),
        vm((2, 2 * rows, 2 * ff), BF16),
        vm((4, rows, width), BF16), vm((2, 4, rows, width // 2), BF16),
        vm((rows, width), BF16), vm((2, rows, width // 2), BF16),
        vm((rows, width), BF16), vm((rows, width), BF16),
        vm((2, rows, width // 2), BF16), vm((2, rows, width // 2), BF16),
        vm((rows, width), BF16),
        vm((4, 8, BLK), F32), vm((3, 4, 8, BLK), F32), vm((2, 8, mix_cols), F32),
        pltpu.SemaphoreType.DMA((len(inputs),)),
        pltpu.SemaphoreType.DMA((N_FAMILIES,)),
        pltpu.SemaphoreType.DMA((N_ARRIVALS,)),
    ]
    summed = pl.pallas_call(
        layer_kernel,
        out_shape=jax.ShapeDtypeStruct(tokens.shape, F32),
        in_specs=[in_hbm] * len(inputs),
        out_specs=on_chip,
        scratch_shapes=scratch,
        compiler_params=pltpu.CompilerParams(
            collective_id=0, has_side_effects=True, vmem_limit_bytes=60 * 1024 * 1024
        ),
    )(*inputs)
    return summed.astype(BF16)


def solution(mesh):
    both = ("fs", "tp")
    in_specs = (
        P(both, None), P(), P(),
        P("fs", "tp"), P("tp"), P("fs", "tp"), P("tp"), P("tp"),
        P(), P(),
        P("tp", "fs"), P("fs"),
        P("fs", "tp"), P("tp"), P("fs", "tp"), P("tp"),
        P("tp", "fs"), P("fs"),
    )
    return jax.shard_map(local, mesh=mesh, in_specs=in_specs, out_specs=P(both, None), check_vma=False)
```

time: 240 us -> 99 us (0.41)
  blocking collectives: 143 us -> 0 us
  Pallas kernels: 0 us -> 96.8 us
  matrix products: 33.5 us -> 0 us
  local copies, waits for them, and re-layouts: 15.9 us -> 0 us
  between operations: 13.6 us -> 0.01 us
  other arithmetic: 13.5 us -> 2.09 us
  waiting for transfers between devices: 10.4 us -> 0 us
  starting transfers between devices: 8.9 us -> 0 us
    all_to_all x7 -> x0, blocking collectives: 118 us -> none  [the longest x2 59.4 us: sum_in_two_steps(): lax.all_to_all(own.astype(jnp.bfloat16), far, 0, 0, tiled=True)]
    pallas_call x0 -> x1, Pallas kernels: none -> 96.8 us  [local(): pl.pallas_call(layer_kernel, out_shape=jax.ShapeDtypeStruct(tokens.shape,...]
    dot_general x6 -> x0, matrix products: 33.5 us -> none  [the longest x1 13.4 us: ffn_term(): jnp.dot(hidden, down_whole, preferred_element_type=jnp.float32)]
    all_gather x1 -> x0, blocking collectives: 24.7 us -> none  [turned_gather(): out, at, finished = (lax.all_gather(both, axis, axis=0, tiled=True), 0, [])]
    all_to_all x2 -> x0, starting transfers between devices: 8.86 us -> none  [copy_for_each(): lax.all_to_all(jnp.broadcast_to(value[None], (peers, *value.shape)), axis...]
    reduce_sum x7 -> x0, other arithmetic: 8.36 us -> none  [the longest x2 7.11 us: sent_and_summed(): return arrived.astype(jnp.float32).sum(axis=0)]
    all_gather x2 -> x0, waiting for transfers between devices: 7.4 us -> none  [turned_gather(): out, at, finished = (lax.all_gather(both, axis, axis=0, tiled=True), 0, [])]
    all_to_all x2 -> x0, local copies, waits for them, and re-layouts: 4.76 us -> none  [copy_for_each(): lax.all_to_all(jnp.broadcast_to(value[None], (peers, *value.shape)), axis...]
  transfers between devices with their start and end apart: 4 -> 0, of which waited for: 3 -> 0; matrix products, arithmetic and copies ran while one was open for 13% -> 0% of each run, Pallas kernels for 0% -> 0%
where the time goes in v2:
time: 99 us; the launch traced here: 98.9 us
  Pallas kernels  96.8 us (98%)
  other arithmetic  2.09 us (2%)
    pallas_call x1, Pallas kernels, local(): pl.pallas_call(layer_kernel, out_shape=jax.ShapeDtypeStruct(tokens.shape,...  96.8 us
    convert_element_type x1, other arithmetic, local(): return summed.astype(BF16)  2.09 us

profile of v2, /device:TPU:0, one launch (start us, length us, event | category | flops | bytes accessed | tf_op | source)
XLA Modules:
  0.0 98.9 jit_solution(10943922426321714636)
XLA Ops:
  0.0 96.8 %shard_map.172 = f32[128,2048]{1,0:T(8,128)} custom-call(bf16[128,2048]{1,0:T(8,128)(2,1)} %refs_0_.1, f32[1,2048]{1,0:T(1,128)} %bitcast.8, f32[128,256]{1,0:T(8,128)} %refs_2_.1, f32[1,256]{1,0:T(1,128)} %bitcast.11, f32[128,256]{1,0:T(8,128)} %refs_4_.1, f32[1,256]{1,0:T(1,128)} %bitcast.12, f32[256,128]{1,0:T(8,128)} %refs_6_.1, f32[1,128]{1,0:T(1,128)} %bitcast.14, ...), custom_call_target="tpu_custom_call" | custom-call | tf_op jit(solution)/shard_map/pallas_call | solution.py:460
  96.8 2.1 %convert_element_type.3 = bf16[128,2048]{1,0:T(8,128)(2,1)} convert(f32[128,2048]{1,0:T(8,128)} %shard_map.172) | non-fusion elementwise | flops 262144 | bytes 1572864 | tf_op jit(solution)/shard_map/convert_element_type | solution.py:470

commit v3 on v2

--- a/solution.py
+++ b/solution.py
@@ -30,44 +30,41 @@
 
 ORDER = (
     184, 187, 185, 186, 235, 0, 1, 20, 21, 4, 5, 24,
-    25, 2000, 136, 168, 1161, 44, 45, 64, 65, 40, 41, 60,
-    61, 1000, 2, 6, 7, 1001, 3, 8, 9, 1012, 22, 26,
-    27, 1013, 23, 28, 29, 1004, 12, 1016, 32, 1028, 1040, 1024,
-    47, 1025, 43, 49, 1036, 67, 1037, 69, 1002, 42, 62, 63,
-    52, 72, 1003, 16, 10, 11, 1110, 188, 1113, 189, 1006, 13,
-    66, 1005, 1018, 33, 1017, 1008, 14, 1014, 68, 1015, 36, 30,
-    31, 1020, 34, 1027, 1029, 46, 1041, 1032, 54, 48, 1026, 56,
-    51, 1038, 1039, 76, 71, 1044, 74, 50, 70, 1009, 15, 18,
-    1042, 73, 1111, 1112, 1007, 17, 1021, 35, 38, 1030, 53, 80,
-    81, 100, 101, 1033, 58, 1045, 78, 1019, 37, 1010, 19, 1031,
-    57, 1043, 77, 1022, 39, 55, 75, 104, 1114, 84, 85, 105,
-    1115, 1011, 1023, 2001, 2002, 1048, 82, 1049, 1061, 2003, 83, 103,
-    86, 1034, 59, 1046, 79, 1060, 2004, 233, 234, 232, 106, 1035,
-    87, 107, 1047, 1064, 1159, 102, 1160, 1052, 1158, 2006, 2008, 204,
-    205, 206, 207, 112, 2005, 2007, 202, 203, 92, 89, 109, 1050,
-    1051, 96, 1063, 1054, 1066, 113, 1130, 93, 91, 1132, 2025, 208,
-    1053, 1062, 116, 111, 1065, 2027, 210, 1131, 1133, 2026, 209, 2028,
-    211, 108, 1056, 94, 88, 1068, 114, 110, 1128, 90, 1129, 1057,
-    98, 95, 1069, 118, 115, 1134, 1136, 2037, 190, 191, 2039, 195,
-    194, 120, 121, 152, 153, 1135, 1137, 2038, 192, 193, 2040, 197,
-    196, 1067, 117, 124, 125, 156, 157, 1116, 198, 1117, 1055, 97,
-    1058, 99, 1070, 119, 1072, 122, 140, 126, 127, 1073, 123, 144,
-    1091, 172, 158, 1092, 176, 1120, 154, 155, 159, 1121, 200, 1095,
-    169, 128, 129, 160, 1076, 137, 1077, 138, 1096, 170, 161, 1074,
-    1118, 199, 1119, 1075, 148, 164, 1059, 130, 131, 1078, 141, 1079,
-    142, 1097, 173, 1093, 1094, 180, 163, 1071, 1098, 174, 162, 133,
-    1122, 1123, 201, 2009, 2010, 1099, 177, 1080, 145, 1081, 146, 134,
-    2011, 132, 165, 1100, 178, 166, 2012, 1124, 1126, 2013, 1103, 171,
-    1082, 149, 1083, 150, 135, 2014, 1102, 182, 167, 1088, 1107, 2021,
-    212, 213, 1101, 181, 1085, 143, 1125, 1127, 2015, 1086, 147, 1090,
-    2016, 1105, 179, 2017, 1104, 175, 1084, 139, 1109, 2018, 1087, 151,
-    2019, 1106, 183, 2020, 2022, 214, 215, 216, 217, 1138, 1139, 1089,
-    1108, 2024, 224, 225, 226, 227, 2023, 222, 223, 1140, 1142, 2029,
-    218, 2031, 220, 1141, 1143, 2030, 219, 2032, 221, 1150, 1152, 2033,
-    228, 2035, 230, 1151, 1153, 2034, 229, 2036, 231, 1148, 1149, 1144,
-    1146, 1145, 1147, 2041, 1154, 1156, 1155, 1157, 2042,
+    25, 2000, 136, 168, 1133, 44, 45, 64, 65, 40, 41, 60,
+    61, 1000, 2, 6, 7, 1001, 3, 8, 9, 1011, 22, 26,
+    27, 1012, 23, 28, 29, 1003, 12, 1014, 32, 1025, 1036, 1022,
+    47, 1023, 43, 49, 1033, 67, 1034, 1102, 188, 42, 62, 63,
+    52, 72, 69, 1104, 189, 1002, 16, 10, 11, 1005, 13, 1004,
+    1016, 33, 1015, 1007, 14, 66, 1013, 36, 30, 31, 1018, 34,
+    1026, 1037, 46, 1029, 54, 1040, 74, 48, 68, 1024, 56, 51,
+    1035, 76, 71, 50, 70, 1103, 1008, 18, 15, 1006, 17, 1019,
+    38, 35, 1038, 73, 1027, 53, 1030, 58, 55, 1017, 37, 1041,
+    78, 75, 1028, 57, 1039, 77, 80, 81, 100, 101, 1009, 19,
+    1105, 1020, 39, 84, 85, 104, 105, 1010, 1021, 2001, 2002, 233,
+    234, 232, 1031, 59, 1042, 79, 1032, 1043, 1044, 82, 86, 87,
+    1055, 107, 1056, 1045, 106, 1132, 2004, 2006, 204, 205, 206, 207,
+    83, 102, 103, 2003, 2005, 202, 203, 1047, 1058, 92, 112, 89,
+    109, 1049, 1048, 1059, 1114, 1116, 2017, 208, 2019, 210, 93, 108,
+    1057, 116, 111, 1060, 1046, 96, 91, 1115, 1117, 2018, 209, 2020,
+    211, 1051, 94, 113, 88, 1062, 114, 1112, 1113, 1052, 98, 95,
+    90, 110, 1063, 118, 115, 1118, 1120, 2029, 190, 191, 2031, 195,
+    194, 1119, 1121, 2030, 192, 193, 2032, 197, 196, 120, 121, 152,
+    153, 1106, 198, 124, 125, 156, 157, 1050, 97, 1053, 99, 1061,
+    117, 1064, 119, 1109, 200, 1066, 122, 140, 126, 127, 1084, 172,
+    159, 1085, 176, 1067, 144, 158, 123, 154, 155, 1108, 199, 128,
+    129, 160, 161, 1069, 137, 1070, 138, 1087, 169, 1088, 170, 1054,
+    1107, 132, 164, 1110, 201, 1071, 141, 1072, 142, 1090, 174, 1068,
+    148, 131, 1086, 180, 163, 1089, 173, 1065, 2007, 133, 165, 2008,
+    2009, 130, 162, 1073, 145, 1074, 146, 134, 1091, 177, 1092, 178,
+    166, 1111, 2010, 1077, 139, 1095, 171, 2011, 1076, 150, 135, 1094,
+    182, 167, 2012, 1078, 143, 1096, 175, 1081, 1099, 2014, 214, 215,
+    216, 217, 2013, 212, 213, 1075, 149, 1079, 147, 1093, 181, 1097,
+    179, 1080, 151, 1098, 183, 1123, 1125, 2021, 218, 2023, 220, 1083,
+    1101, 1124, 1126, 2022, 219, 2024, 221, 1082, 1100, 2016, 224, 225,
+    226, 227, 2015, 222, 223, 1122, 2033, 1128, 1130, 2025, 228, 2027,
+    230, 1129, 1131, 2026, 229, 2028, 231, 1127, 2034,
 )
-N_FAMILIES, N_ARRIVALS = 31, 162
+N_FAMILIES, N_ARRIVALS = 19, 134
 
 
 COLUMNS = (
@@ -121,6 +118,8 @@
 
 def arrival_group(name):
     head, _, key = name.partition(":")
+    if key[:2] == "1f":
+        return head, "1f", 1
     if key[0] == "e":
         early = key[1] != "P" and key[2] != "2"
         return (head, "ea", 9) if early else (head, "eb", 4) if key[2] == "2" else (head, "ec", 3)
@@ -133,7 +132,7 @@
             return head, "2a", 2
         if key in ("2o-", "2L-"):
             return head, "2b", 2
-    return head, key, 1
+    return head, key, 0
 
 
 def layer_kernel(
@@ -244,23 +243,24 @@
     col_ids = lax.broadcasted_iota(jnp.int32, (BLK, BLK), 1)
     eye = row_ids == col_ids
 
-    def project_mixer(first, core):
+    def project_mixer(first):
         rows = x1[first : first + 2].reshape(2 * BLK, -1)
-        cols = slice(core * 256, core * 256 + 256)
-        u = gelu(jnp.dot(rows, ub[core].reshape(A, 256), preferred_element_type=F32))
-        v = gelu(jnp.dot(rows, vb[core].reshape(A, 256), preferred_element_type=F32)).astype(BF16)
-        u_val[first : first + 2, :, cols] = u.astype(BF16).reshape(2, BLK, 256)
-        v_val[first : first + 2, :, cols] = v.reshape(2, BLK, 256)
-        wide = v.astype(F32)
-        columns = jnp.sum(wide, axis=1, keepdims=True), jnp.sum(wide * wide, axis=1, keepdims=True)
+        sums = squares = 0.0
+        for core in range(2):
+            cols = slice(core * 256, core * 256 + 256)
+            u = gelu(jnp.dot(rows, ub[core].reshape(A, 256), preferred_element_type=F32))
+            v = gelu(jnp.dot(rows, vb[core].reshape(A, 256), preferred_element_type=F32)).astype(BF16)
+            u_val[first : first + 2, :, cols] = u.astype(BF16).reshape(2, BLK, 256)
+            v_val[first : first + 2, :, cols] = v.reshape(2, BLK, 256)
+            wide = v.astype(F32)
+            sums = sums + jnp.sum(wide, axis=1, keepdims=True)
+            squares = squares + jnp.sum(wide * wide, axis=1, keepdims=True)
         for k in range(2):
-            chip = slot_chip[first + k]
-            for row in range(2):
-                piece = columns[row][k * BLK : (k + 1) * BLK]
-                turned = jnp.sum(jnp.where(eye, piece, 0.0), axis=0, keepdims=True)
-                if core == 1:
-                    turned = turned + stat[chip, row : row + 1, :]
-                stat[chip, row : row + 1, :] = turned
+            for row, column in ((0, sums), (1, squares)):
+                piece = column[k * BLK : (k + 1) * BLK]
+                stat[slot_chip[first + k], row : row + 1, :] = jnp.sum(
+                    jnp.where(eye, piece, 0.0), axis=0, keepdims=True
+                )
 
     def mixing_rows(core):
         masked = jnp.where(col_ids <= row_ids, spatial[2 * y + core].astype(F32), 0.0)
@@ -296,13 +296,14 @@
             total = jnp.dot(rows, matrix, preferred_element_type=F32)
             part1[first : first + 2, :, j * 256 : j * 256 + 256] = total.astype(BF16).reshape(2, BLK, 256)
 
-    def project_ffn(first, n):
+    def project_ffn(first, part):
         rows = x2[first : first + 2].reshape(2 * BLK, -1)
-        core, j = n // 3, n % 3
-        cols = slice(j * 256, j * 256 + 256)
-        gate = jnp.dot(rows, gb[core, :, :, :, cols].reshape(A, 256), preferred_element_type=F32)
-        up = jnp.dot(rows, pb[core, :, :, :, cols].reshape(A, 256), preferred_element_type=F32)
-        hid[first // 2, :, n * 256 : n * 256 + 256] = (silu(gate) * up).astype(BF16)
+        for n in (2 * part, 2 * part + 1):
+            core, j = n // 3, n % 3
+            cols = slice(j * 256, j * 256 + 256)
+            gate = jnp.dot(rows, gb[core, :, :, :, cols].reshape(A, 256), preferred_element_type=F32)
+            up = jnp.dot(rows, pb[core, :, :, :, cols].reshape(A, 256), preferred_element_type=F32)
+            hid[first // 2, :, n * 256 : n * 256 + 256] = (silu(gate) * up).astype(BF16)
 
     def place_of(dz, dx):
         return lax.rem(z + dz + 4, 4), lax.rem(x + dx + 4, 4)
@@ -337,7 +338,7 @@
             held = slice(j * BLK, j * BLK + BLK)
             total = res[:, cols].astype(F32) + part2[part, OWN, :, held].astype(F32)
             total = total + fl2[part, :, held].astype(F32) + fr2[part, :, held].astype(F32)
-            out_ref[:, cols] = total
+            out_ref[:, cols] = total.astype(BF16)
 
     def convert_rest():
         ready(14)
@@ -351,10 +352,10 @@
 
     halves = (LEFT, OPP)
     work = [convert_rest]
-    work += [functools.partial(project_mixer, first, core) for first in halves for core in range(2)]
+    work += [functools.partial(project_mixer, first) for first in halves]
     work += [lambda: (mix(LEFT), mix(RIGHT)), lambda: (mix(OPP), mix(OWN))]
     work += [functools.partial(project_out, first) for first in halves]
-    work += [functools.partial(project_ffn, first, n) for first in halves for n in range(6)]
+    work += [functools.partial(project_ffn, first, n) for first in halves for n in range(3)]
     work += [functools.partial(project_down, first, part) for part in range(2) for first in halves]
     for part, relay in ((part1, relay1), (part2.at[0], relay2.at[0]), (part2.at[1], relay2.at[1])):
         work += [functools.partial(add_relayed, part, relay, q) for q in range(4)]
@@ -362,10 +363,10 @@
     work += [functools.partial(finish, part) for part in range(2)]
 
     families = {}
-    for n, buf in (("U", ub), ("V", vb), ("OA", oab), ("OB", obb), ("G", gb), ("Q", pb), ("DA", dab), ("DB", dbb)):
-        families[n + "1"] = buf.at[0, 0, pl.ds(0, 3)]
-        families[n + "2"] = buf.at[0, pl.ds(0, 3)]
-        families[n + "s"] = buf.at[0]
+    for n, buf in (("U", ub), ("O", oab), ("G", gb), ("D", dab)):
+        families[n + "1"] = buf.at[:, 0, pl.ds(0, 3)]
+        families[n + "2"] = buf.at[:, pl.ds(0, 3)]
+        families[n + "s"] = buf
     families["X1"], families["X2"], families["S1"] = x1.at[pl.ds(0, 3)], x2.at[pl.ds(0, 3)], part1.at[pl.ds(0, 3)]
     families["S2"], families["S3"] = part2.at[0, pl.ds(0, 3)], part2.at[1, pl.ds(0, 3)]
     families["stat"], families["vg"] = stat_in, vg.at[0]
@@ -375,10 +376,21 @@
         head, _, tail = name.partition(":")
         if head in families:
             return head
-        return head + (tail[0] if tail[0] in "12" else "s")
+        kin = {"V": "U", "Q": "G"}.get(head, head[0])
+        return kin + (tail[0] if tail[0] in "12" else "s")
 
     buffers = {"U": ub, "V": vb, "OA": oab, "OB": obb, "G": gb, "Q": pb, "DA": dab, "DB": dbb}
     arrivals, arrival_of = [], {}
+    together = [
+        (n, part2.at[0, pl.ds(0, 2)], [k for k in moves if k[:2] == f"S{n}" and k[3] in "nr"]) for n in (2, 3)
+    ]
+    together += [
+        (4, x2.at[0], ("X2:0-", "X2:2+", "X2:1-", "X2:3+")),
+        (5, x2.at[0], [f"X2:f{q}" for q in range(4)]),
+        (6, x1.at[0], ("X1:H0-", "X1:H1+")),
+        (7, x1.at[0], ("X1:f+", "X1:f-")),
+        (8, stat_in, ("stat:R", "stat:L", "stat:P")),
+    ]
     known = {}
     for name, (_, _, to, ref) in moves.items():
         head = name.partition(":")[0]
@@ -386,9 +398,13 @@
         if head in buffers:
             key = arrival_group(name)
             buf, blocks = buffers[head], key[2]
-            if blocks > 1:
+            if blocks:
                 ref = {16: buf.at[0], 9: buf.at[0, pl.ds(0, 3), pl.ds(0, 3)]}.get(blocks)
                 ref = buf.at[0, 0, pl.ds(0, blocks)] if ref is None else ref
+        else:
+            for key_of, ref_of, members in together:
+                if name in members:
+                    key, ref = key_of, ref_of
         if key not in known:
             known[key] = len(arrivals)
             arrivals.append((ref, to))
@@ -457,9 +473,9 @@
         pltpu.SemaphoreType.DMA((N_FAMILIES,)),
         pltpu.SemaphoreType.DMA((N_ARRIVALS,)),
     ]
-    summed = pl.pallas_call(
+    return pl.pallas_call(
         layer_kernel,
-        out_shape=jax.ShapeDtypeStruct(tokens.shape, F32),
+        out_shape=jax.ShapeDtypeStruct(tokens.shape, BF16),
         in_specs=[in_hbm] * len(inputs),
         out_specs=on_chip,
         scratch_shapes=scratch,
@@ -467,7 +483,6 @@
             collective_id=0, has_side_effects=True, vmem_limit_bytes=60 * 1024 * 1024
         ),
     )(*inputs)
-    return summed.astype(BF16)
 
 
 def solution(mesh):

time: 99 us -> 97.2 us (0.982)
  other arithmetic: 2.09 us -> 0 us
  local copies, waits for them, and re-layouts: 0 us -> 1.88 us
  Pallas kernels: 96.8 us -> 95.2 us
    convert_element_type x1 -> x0, other arithmetic: 2.09 us -> none  [local(): return summed.astype(BF16)]
    unnamed x0 -> x1, local copies, waits for them, and re-layouts: none -> 1.88 us
    pallas_call x1, Pallas kernels: 96.8 us -> 95.2 us  [local(): pl.pallas_call(layer_kernel, out_shape=jax.ShapeDtypeStruct(tokens.shape,...]
where the time goes in v3:
time: 97.2 us; the launch traced here: 97.1 us
  Pallas kernels  95.2 us (98%)
  local copies, waits for them, and re-layouts  1.88 us (2%)
    pallas_call x1, Pallas kernels, local(): pl.pallas_call(layer_kernel, out_shape=jax.ShapeDtypeStruct(tokens.shape,...  95.2 us

profile of v3, /device:TPU:0, one launch (start us, length us, event | category | flops | bytes accessed | tf_op | source)
XLA Modules:
  0.0 97.1 jit_solution(3615660086468761870)
XLA Ops:
  0.0 95.2 %shard_map.172 = bf16[128,2048]{1,0:T(8,128)(2,1)} custom-call(bf16[128,2048]{1,0:T(8,128)(2,1)} %refs_0_.1, f32[1,2048]{1,0:T(1,128)} %bitcast.8, f32[128,256]{1,0:T(8,128)} %refs_2_.1, f32[1,256]{1,0:T(1,128)} %bitcast.11, f32[128,256]{1,0:T(8,128)} %refs_4_.1, f32[1,256]{1,0:T(1,128)} %bitcast.12, f32[256,128]{1,0:T(8,128)} %refs_6_.1, ...), custom_call_target="tpu_custom_call" | custom-call | tf_op jit(solution)/shard_map/pallas_call | solution.py:476
  95.2 1.9 %copy.20 = bf16[128,2048]{1,0:T(8,128)(2,1)} copy(bf16[128,2048]{1,0:T(8,128)(2,1)} %shard_map.172) | data formatting | bytes 1048576

commit v4 on v3

--- a/solution.py
+++ b/solution.py
@@ -40,29 +40,29 @@
     1035, 76, 71, 50, 70, 1103, 1008, 18, 15, 1006, 17, 1019,
     38, 35, 1038, 73, 1027, 53, 1030, 58, 55, 1017, 37, 1041,
     78, 75, 1028, 57, 1039, 77, 80, 81, 100, 101, 1009, 19,
-    1105, 1020, 39, 84, 85, 104, 105, 1010, 1021, 2001, 2002, 233,
-    234, 232, 1031, 59, 1042, 79, 1032, 1043, 1044, 82, 86, 87,
-    1055, 107, 1056, 1045, 106, 1132, 2004, 2006, 204, 205, 206, 207,
-    83, 102, 103, 2003, 2005, 202, 203, 1047, 1058, 92, 112, 89,
-    109, 1049, 1048, 1059, 1114, 1116, 2017, 208, 2019, 210, 93, 108,
-    1057, 116, 111, 1060, 1046, 96, 91, 1115, 1117, 2018, 209, 2020,
-    211, 1051, 94, 113, 88, 1062, 114, 1112, 1113, 1052, 98, 95,
-    90, 110, 1063, 118, 115, 1118, 1120, 2029, 190, 191, 2031, 195,
-    194, 1119, 1121, 2030, 192, 193, 2032, 197, 196, 120, 121, 152,
-    153, 1106, 198, 124, 125, 156, 157, 1050, 97, 1053, 99, 1061,
-    117, 1064, 119, 1109, 200, 1066, 122, 140, 126, 127, 1084, 172,
-    159, 1085, 176, 1067, 144, 158, 123, 154, 155, 1108, 199, 128,
-    129, 160, 161, 1069, 137, 1070, 138, 1087, 169, 1088, 170, 1054,
-    1107, 132, 164, 1110, 201, 1071, 141, 1072, 142, 1090, 174, 1068,
-    148, 131, 1086, 180, 163, 1089, 173, 1065, 2007, 133, 165, 2008,
-    2009, 130, 162, 1073, 145, 1074, 146, 134, 1091, 177, 1092, 178,
-    166, 1111, 2010, 1077, 139, 1095, 171, 2011, 1076, 150, 135, 1094,
-    182, 167, 2012, 1078, 143, 1096, 175, 1081, 1099, 2014, 214, 215,
-    216, 217, 2013, 212, 213, 1075, 149, 1079, 147, 1093, 181, 1097,
-    179, 1080, 151, 1098, 183, 1123, 1125, 2021, 218, 2023, 220, 1083,
-    1101, 1124, 1126, 2022, 219, 2024, 221, 1082, 1100, 2016, 224, 225,
-    226, 227, 2015, 222, 223, 1122, 2033, 1128, 1130, 2025, 228, 2027,
-    230, 1129, 1131, 2026, 229, 2028, 231, 1127, 2034,
+    84, 85, 104, 105, 1105, 1020, 39, 1010, 1021, 2001, 2002, 233,
+    234, 232, 1031, 59, 1042, 79, 120, 121, 152, 153, 1032, 1043,
+    1044, 82, 86, 87, 1055, 107, 1056, 1045, 106, 1132, 2004, 2006,
+    204, 205, 206, 207, 83, 102, 103, 2003, 2005, 202, 203, 1047,
+    1058, 1066, 92, 112, 89, 109, 140, 1084, 172, 1085, 176, 1067,
+    144, 1114, 1116, 2017, 208, 2019, 210, 1049, 93, 108, 1048, 1059,
+    1115, 155, 1117, 2018, 209, 123, 2020, 211, 1057, 116, 111, 1060,
+    1046, 96, 91, 113, 88, 1051, 94, 1062, 114, 1112, 1113, 1118,
+    90, 110, 1120, 2029, 190, 191, 2031, 195, 194, 1052, 98, 95,
+    1063, 118, 115, 1119, 1121, 2030, 192, 193, 2032, 197, 196, 122,
+    154, 1106, 198, 124, 125, 156, 157, 126, 127, 158, 159, 1109,
+    200, 1050, 97, 1061, 117, 1068, 148, 128, 129, 160, 161, 1086,
+    180, 1053, 99, 1064, 119, 1108, 199, 1069, 137, 132, 131, 162,
+    163, 1070, 138, 1087, 169, 1088, 170, 1107, 164, 130, 1110, 201,
+    1071, 141, 1072, 142, 1089, 173, 1090, 174, 1054, 133, 165, 1073,
+    145, 1074, 146, 134, 1091, 177, 1092, 178, 166, 1065, 2007, 2008,
+    2009, 1076, 150, 135, 1077, 139, 1093, 181, 1094, 182, 167, 1111,
+    2010, 1081, 1099, 2011, 1075, 149, 1095, 171, 2012, 1079, 147, 1097,
+    179, 1078, 143, 1096, 175, 2014, 214, 215, 216, 217, 2013, 212,
+    213, 1101, 1083, 1080, 151, 1098, 183, 1123, 1125, 2021, 218, 2023,
+    220, 1082, 1100, 2016, 224, 225, 226, 227, 2015, 222, 223, 1124,
+    1126, 2022, 219, 2024, 221, 1128, 1130, 2025, 228, 2027, 230, 1129,
+    1131, 2026, 229, 2028, 231, 1122, 2033, 1127, 2034,
 )
 N_FAMILIES, N_ARRIVALS = 19, 134
 

time: 97.2 us -> 99.3 us (1.022)
  Pallas kernels: 95.2 us -> 97.2 us
    pallas_call x1, Pallas kernels: 95.2 us -> 97.2 us  [local(): pl.pallas_call(layer_kernel, out_shape=jax.ShapeDtypeStruct(tokens.shape,...]
where the time goes in v4:
time: 99.3 us; the launch traced here: 99.1 us
  Pallas kernels  97.2 us (98%)
  local copies, waits for them, and re-layouts  1.88 us (2%)
    pallas_call x1, Pallas kernels, local(): pl.pallas_call(layer_kernel, out_shape=jax.ShapeDtypeStruct(tokens.shape,...  97.2 us

profile of v4, /device:TPU:0, one launch (start us, length us, event | category | flops | bytes accessed | tf_op | source)
XLA Modules:
  0.0 99.1 jit_solution(11402824232011218599)
XLA Ops:
  0.0 97.2 %shard_map.172 = bf16[128,2048]{1,0:T(8,128)(2,1)} custom-call(bf16[128,2048]{1,0:T(8,128)(2,1)} %refs_0_.1, f32[1,2048]{1,0:T(1,128)} %bitcast.8, f32[128,256]{1,0:T(8,128)} %refs_2_.1, f32[1,256]{1,0:T(1,128)} %bitcast.11, f32[128,256]{1,0:T(8,128)} %refs_4_.1, f32[1,256]{1,0:T(1,128)} %bitcast.12, f32[256,128]{1,0:T(8,128)} %refs_6_.1, ...), custom_call_target="tpu_custom_call" | custom-call | tf_op jit(solution)/shard_map/pallas_call | solution.py:476
  97.2 1.9 %copy.20 = bf16[128,2048]{1,0:T(8,128)(2,1)} copy(bf16[128,2048]{1,0:T(8,128)(2,1)} %shard_map.172) | data formatting | bytes 1048576
